TPU v7x, 32 devices: a whole 2x2x4 slice. The times are simulated.
32 devices in a mesh: sp: 8 (over z, y), tp: 4 (over x, core).
Axes of the slice: x: 2, y: 2, z: 4, core: 2. Of those that a mesh axis runs over, the one named last changes fastest.
Arguments:
- residual: bfloat16 [5120, 2048], P('sp', 'tp'), may hold values from -4 to 4
- query_wide: bfloat16 [5120, 1536], P('sp', 'tp'), may hold values from -500 to 500
- query_narrow: bfloat16 [5120, 1024], P('sp', 'tp'), may hold values from -500 to 500
- latent: bfloat16 [5120, 512], P('sp'), may hold values from -6 to 6
- rope_key: bfloat16 [5120, 64], P('sp'), may hold values from -6 to 6
- latent_gain: float32 [512], replicated, may hold values from 0.1 to 1.9
- expand_wide: bfloat16 [512, 2048], P(None, 'tp'), may hold values from -0.25 to 0.25
- expand_narrow: bfloat16 [512, 1024], P(None, 'tp'), may hold values from -0.25 to 0.25
- out_wide: bfloat16 [1024, 2048], P('tp'), may hold values from -0.1875 to 0.1875
- out_narrow: bfloat16 [512, 2048], P('tp'), may hold values from -0.25 to 0.25
- norm_gain: float32 [2048], P('tp'), may hold values from 0.1 to 1.9
- up_gate: bfloat16 [2048, 5632], P('sp', 'tp'), may hold values from -0.125 to 0.125
- up_value: bfloat16 [2048, 5632], P('sp', 'tp'), may hold values from -0.125 to 0.125
- down_weight: bfloat16 [2048, 5632], P('sp', 'tp'), may hold values from -0.078125 to 0.078125
- conv_taps: float32 [3, 2, 5632], P(None, None, 'tp'), may hold values from -3 to 3
Outputs:
- output: bfloat16 [5120, 2048], P('sp', 'tp')
All inputs are finite; a program needn't handle non-finite values.
Results may differ from a plain program's by a relative error of at most 0.025.
Values may be sent and summed in bfloat16 or wider, within the bound.
No kernel may reach another device: no remote copies, remote signals or barrier semaphores. Data moves between devices by JAX's collectives and lax.ppermute only.
A program may use at most 192 MiB of HBM per device.

v0:
```python
import functools

import jax
import jax.numpy as jnp
from jax import lax
from jax.experimental import pallas as pl
from jax.experimental.pallas import tpu as pltpu
from jax.sharding import PartitionSpec as P


ROPE = 64
NOPE_W = 128
VAL_W = 128
NOPE_N = 64
VAL_N = 64
LANES = 128

theta = 10000.0
epsilon = 1e-06
F32 = jnp.float32
BF16 = jnp.bfloat16
LOG2E = 1.4426950408889634


def angles_of(positions):
    half_dim = ROPE // 2
    inverse = jnp.power(jnp.float32(theta), -2.0 * jnp.arange(half_dim, dtype=jnp.float32) / ROPE)
    angles = positions[:, None] * inverse[None, :]
    return jnp.cos(angles), jnp.sin(angles)


def rotate(values, cosine, sine):
    half_dim = values.shape[-1] // 2
    floats = values.astype(jnp.float32)
    lower_half = floats[..., :half_dim]
    upper_half = floats[..., half_dim:]
    turned = jnp.concatenate(
        [
            lower_half * cosine - upper_half * sine,
            lower_half * sine + upper_half * cosine,
        ],
        axis=-1,
    )
    return turned.astype(jnp.bfloat16)


def gather_in(pieces, target, offsets, sems):
    copies = []
    for i, (piece, at) in enumerate(zip(pieces, offsets)):
        copy = pltpu.make_async_copy(piece, target.at[pl.ds(at, piece.shape[0])], sems.at[i])
        copy.start()
        copies.append(copy)
    return copies


def attention_kernel(wide, heads, odd, pick, factor, rows, tile, passes, *refs):
    scratch = 10 if passes else 9
    q_ref, c_ref, n_ref, e_ref, *pieces = refs[:-scratch]
    o_ref, lat, q_scr, kv_ref, s_scr, m_scr, l_scr, a_scr, sems = (refs[-10:-9] + refs[-8:]) if passes else refs[-9:]
    width = q_scr.shape[1] // heads
    blocks = q_ref.shape[0] // rows
    key_count = kv_ref.shape[0]
    rank = e_ref.shape[0]
    tiles = key_count // tile
    groups = tile // LANES
    scale = factor * LOG2E
    value_base = heads * width
    total = heads * blocks

    def fetch(j):
        at = pl.ds(pl.multiple_of(j * tile, tile), tile)
        return pltpu.make_async_copy(pieces[0].at[at], lat.at[at], sems.at[j])

    offsets, at = [], 0
    for piece in pieces:
        offsets.append(at)
        at += piece.shape[0]
    if len(pieces) > 1:
        copies = gather_in(pieces, lat, offsets, sems)
    else:
        copies = []
        for j in range(tiles):
            fetch(j).start()

    def turn(values):
        lane = lax.broadcasted_iota(jnp.int32, values.shape, 1)
        quarter = ROPE // 2
        swapped = jnp.where(
            (lane // quarter) % 2 == 0,
            pltpu.roll(values, LANES - quarter, 1),
            pltpu.roll(values, quarter, 1),
        )
        return (values * c_ref[...] + swapped * n_ref[...]).astype(BF16)

    queries = q_ref[...].astype(F32)
    for h in range(heads):
        if wide:
            head = NOPE_W + ROPE
            full = queries.shape[1]
            if full < 2 * LANES:
                shifted = jnp.concatenate([queries, jnp.zeros((queries.shape[0], 2 * LANES - full), F32)], axis=1)
            else:
                shifted = queries if h + pick == 0 else pltpu.roll(queries, full - (h + pick) * head, 1)
            q_scr[:, h * width : h * width + LANES] = shifted[:, :LANES].astype(BF16)
            q_scr[:, h * width + LANES : (h + 1) * width] = turn(shifted[:, LANES : 2 * LANES])
        else:
            q_scr[:, h * width : (h + 1) * width] = turn(queries[:, h * width : (h + 1) * width])

    for copy in copies:
        copy.wait()
    if passes:
        onward = pltpu.make_async_copy(lat, refs[-9], sems.at[len(pieces)])
        onward.start()

    def expand(j, c):
        at = pl.multiple_of(j * tile, tile)
        if not copies:
            fetch(j).wait()
        x = lat[pl.ds(at, tile), :rank]
        rope = lat[pl.ds(at, tile), rank:].astype(F32)
        lane = lax.broadcasted_iota(jnp.int32, rope.shape, 1)
        for h in range(heads):
            if wide:
                both = NOPE_W + VAL_W
                kv = jnp.dot(x, e_ref[:, (h + pick) * both : (h + pick + 1) * both], preferred_element_type=F32).astype(BF16)
                kv_ref[pl.ds(at, tile), h * width : h * width + LANES] = kv[:, :LANES]
                kv_ref[pl.ds(at, tile), h * width + LANES : (h + 1) * width] = jnp.where(
                    lane < ROPE, rope, 0.0
                ).astype(BF16)
                v_at = value_base + h * LANES
                kv_ref[pl.ds(at, tile), v_at : v_at + LANES] = kv[:, LANES:]
            else:
                kv = jnp.dot(x, e_ref[...], preferred_element_type=F32)
                kv_ref[pl.ds(at, tile), :LANES] = jnp.where(lane < NOPE_N, kv, rope).astype(BF16)
                kv_ref[pl.ds(at, tile), LANES:] = kv.astype(BF16)
        return c

    lax.fori_loop(0, tiles, expand, 0)

    def place(b):
        h = b // blocks
        return h, pl.multiple_of((b - h * blocks) * rows, rows)

    def score(b, buf, j):
        h, r = place(b)
        q = q_scr[pl.ds(r, rows), pl.ds(pl.multiple_of(h * width, LANES), width)]
        at = pl.multiple_of(j * tile, tile)
        k = kv_ref[pl.ds(at, tile), pl.ds(pl.multiple_of(h * width, LANES), width)]
        s = lax.dot_general(q, k, (((1,), (1,)), ((), ())), preferred_element_type=F32)
        s_scr[buf, :, pl.ds(at, tile)] = s
        top = s[:, :LANES]
        for g in range(1, groups):
            top = jnp.maximum(top, s[:, g * LANES : (g + 1) * LANES])
        m_scr[buf] = jnp.maximum(m_scr[buf], top)

    def weigh(b, buf, j):
        h, _ = place(b)
        at = pl.multiple_of(j * tile, tile)
        v_at = pl.multiple_of(value_base + h * LANES, LANES)
        v = kv_ref[pl.ds(at, tile), pl.ds(v_at, LANES)]
        top = m_scr[buf]
        low = []
        part = None
        for g in range(groups):
            s = s_scr[buf, :, pl.ds(pl.multiple_of(at + g * LANES, LANES), LANES)]
            p = jnp.exp2((s - top) * scale)
            part = p if part is None else part + p
            low.append(p.astype(BF16))
        l_scr[...] += part
        a_scr[...] += jnp.dot(jnp.concatenate(low, axis=1), v, preferred_element_type=F32)

    def write(b):
        h, r = place(b)
        out = a_scr[...] / jnp.sum(l_scr[...], axis=1, keepdims=True)
        if not wide:
            lane = lax.broadcasted_iota(jnp.int32, (rows, LANES), 1)
            if odd:
                out = jnp.where(lane >= VAL_N, out, 0.0)
            else:
                out = jnp.where(lane < VAL_N, pltpu.roll(out, VAL_N, 1), 0.0)
        o_ref[pl.ds(r, rows), pl.ds(pl.multiple_of(h * LANES, LANES), LANES)] = out.astype(BF16)

    def clear_max(buf):
        m_scr[buf] = jnp.full((rows, LANES), -jnp.inf, F32)

    clear_max(0)

    def first(j, c):
        score(0, 0, j)
        return c

    lax.fori_loop(0, tiles, first, 0)

    def step(b, c):
        buf = lax.rem(b, 2)
        m_scr[buf] = jnp.broadcast_to(jnp.max(m_scr[buf], axis=1, keepdims=True), (rows, LANES))
        clear_max(1 - buf)
        l_scr[...] = jnp.zeros_like(l_scr)
        a_scr[...] = jnp.zeros_like(a_scr)
        after = jnp.minimum(b + 1, total - 1)

        def both(j, c):
            score(after, 1 - buf, j)
            weigh(b, buf, j)
            return c

        lax.fori_loop(0, tiles, both, 0)
        write(b)
        return c

    lax.fori_loop(0, total, step, 0)
    if passes:
        onward.wait()


VMEM_SPEC = pl.BlockSpec(memory_space=pltpu.VMEM)
SMEM_SPEC = pl.BlockSpec(memory_space=pltpu.SMEM)
HBM_SPEC = pl.BlockSpec(memory_space=pltpu.HBM)
ANY_SPEC = pl.BlockSpec(memory_space=pl.ANY)


def attend(query, tables, weights, pieces, heads, wide, odd, factor, passes=False, pick=0):
    tok = query.shape[0]
    keys = sum(p.shape[0] for p in pieces)
    rows = tok // 2 if tok % 32 == 0 else tok
    tile = 1024 if keys % 1024 == 0 else keys
    width = 2 * LANES if wide else LANES
    out = jax.ShapeDtypeStruct((tok, heads * LANES), BF16)
    kept = jax.ShapeDtypeStruct((keys, pieces[0].shape[1]), BF16)
    return pl.pallas_call(
        functools.partial(attention_kernel, wide, heads, odd, pick, factor, rows, tile, passes),
        out_shape=(out, kept) if passes else out,
        in_specs=[VMEM_SPEC] * 4 + [ANY_SPEC if passes else HBM_SPEC] * len(pieces),
        out_specs=(VMEM_SPEC, HBM_SPEC) if passes else VMEM_SPEC,
        scratch_shapes=[
            pltpu.VMEM((keys, pieces[0].shape[1]), BF16),
            pltpu.VMEM((tok, heads * width), BF16),
            pltpu.VMEM((keys, heads * (width + LANES)), BF16),
            pltpu.VMEM((2, rows, keys), F32),
            pltpu.VMEM((2, rows, LANES), F32),
            pltpu.VMEM((rows, LANES), F32),
            pltpu.VMEM((rows, LANES), F32),
            pltpu.SemaphoreType.DMA((max(len(pieces), keys // tile) + 1,)),
        ],
        compiler_params=pltpu.CompilerParams(vmem_limit_bytes=60 * 2**20),
        cost_estimate=pl.CostEstimate(flops=2 * tok * keys * heads * (width + LANES), bytes_accessed=keys * 1024, transcendentals=0),
    )(query, *tables, weights, *pieces)


def base_kernel(n, heads, first, *refs):
    xs, weights = refs[:heads], refs[heads : heads + n]
    o_ref, w_scr, sems = refs[heads + n :]
    depth = weights[0].shape[0] // heads
    total = o_ref.shape[0]
    parts = [w.at[pl.ds(h * depth, depth)] for h in range(heads) for w in weights]
    for copy in gather_in(parts, w_scr, [i * depth for i in range(heads * n)], sems):
        copy.wait()
    rows = 320 if total % 320 == 0 else total

    def multiply(i, c):
        r = pl.multiple_of(i * rows, rows)
        out = None
        for h, x_ref in enumerate(xs):
            part = jnp.dot(
                x_ref[pl.ds(first + r, rows), :],
                w_scr[h * n * depth : (h + 1) * n * depth, :],
                preferred_element_type=F32,
            )
            out = part if out is None else out + part
        o_ref[pl.ds(r, rows), :] = out.astype(BF16)
        return c

    lax.fori_loop(0, total // rows, multiply, 0)


def project_base(xs, weights, first, total):
    n, heads = len(weights), len(xs)
    depth, width = weights[0].shape
    return pl.pallas_call(
        functools.partial(base_kernel, n, heads, first),
        out_shape=jax.ShapeDtypeStruct((total, width), BF16),
        in_specs=[VMEM_SPEC] * heads + [HBM_SPEC] * n,
        out_specs=VMEM_SPEC,
        scratch_shapes=[
            pltpu.VMEM((n * depth, width), BF16),
            pltpu.SemaphoreType.DMA((heads * n,)),
        ],
        compiler_params=pltpu.CompilerParams(vmem_limit_bytes=20 * 2**20),
        cost_estimate=pl.CostEstimate(flops=2 * total * n * depth * width, bytes_accessed=10**6, transcendentals=0),
        name="project_base",
    )(*xs, *weights)


def norm_kernel(n, s_ref, *refs):
    bases, (x_ref, g_ref) = refs[:2], refs[2:4]
    weights, residuals = refs[4 : 4 + n], refs[4 + n : 4 + 2 * n]
    a_ref, out_ref, edge_ref, o_ref, w_scr, r_scr, y_scr, sems, sems_r, sems_o = refs[4 + 2 * n :]
    depth = weights[0].shape[0]
    total, width = bases[0].shape
    copies = gather_in(weights, w_scr, [i * depth for i in range(n)], sems)
    more = gather_in(residuals, r_scr, [i * 2 * total for i in range(n)], sems_r)
    for copy in copies + more:
        copy.wait()
    rows = 128 if total % 128 == 0 else total
    own = r_scr.shape[1]
    mine = pl.ds(pl.multiple_of(s_ref[n], own), own)

    def put(i):
        at = pl.ds(pl.multiple_of(i * rows, rows), rows)
        return pltpu.make_async_copy(o_ref.at[at], out_ref.at[at], sems_o.at[i])

    for half, b_ref in enumerate(bases):

        def multiply(i, c, half=half, b_ref=b_ref):
            r = pl.multiple_of(i * rows, rows)
            at = pl.multiple_of(half * total + r, rows)
            for p in range(n):
                lanes = pl.ds(pl.multiple_of(s_ref[p], own), own)
                res = r_scr[pl.ds(pl.multiple_of(p * 2 * total + at, rows), rows), :]
                y_scr[:, lanes] = res.astype(F32)
            y = b_ref[pl.ds(r, rows), :].astype(F32) + jnp.dot(
                x_ref[pl.ds(at, rows), :], w_scr[...], preferred_element_type=F32
            )
            y = (y + y_scr[...]).astype(BF16).astype(F32)
            y_scr[...] = y

            @pl.when(s_ref[n + 1] == half)
            def _():
                a_ref[pl.ds(r, rows), :] = y_scr[:, mine].astype(BF16)

            mean = jnp.sum(y * y, axis=1, keepdims=True) * (1.0 / width)
            o_ref[pl.ds(at, rows), :] = (y * lax.rsqrt(mean + epsilon) * g_ref[...]).astype(BF16)
            put(half * (total // rows) + i).start()
            return c

        lax.fori_loop(0, total // rows, multiply, 0)
    edge_ref[0:16, :] = o_ref[0:16, :]
    edge_ref[16:32, :] = o_ref[2 * total - 16 : 2 * total, :]
    for i in range(2 * total // rows):
        put(i).wait()


def project_norm(places, bases, x, gain, weights, residuals):
    total, width = bases[0].shape
    n = len(weights)
    own = residuals[0].shape[1]
    rows = 128 if total % 128 == 0 else total
    return pl.pallas_call(
        functools.partial(norm_kernel, n),
        out_shape=(
            jax.ShapeDtypeStruct((total, own), BF16),
            jax.ShapeDtypeStruct((2 * total, width), BF16),
            jax.ShapeDtypeStruct((32, width), BF16),
        ),
        in_specs=[SMEM_SPEC] + [VMEM_SPEC] * 4 + [HBM_SPEC] * (2 * n),
        out_specs=(VMEM_SPEC, HBM_SPEC, VMEM_SPEC),
        scratch_shapes=[
            pltpu.VMEM((2 * total, width), BF16),
            pltpu.VMEM((n * weights[0].shape[0], width), BF16),
            pltpu.VMEM((n * 2 * total, own), BF16),
            pltpu.VMEM((rows, width), F32),
            pltpu.SemaphoreType.DMA((n,)),
            pltpu.SemaphoreType.DMA((n,)),
            pltpu.SemaphoreType.DMA((2 * total // rows,)),
        ],
        compiler_params=pltpu.CompilerParams(vmem_limit_bytes=28 * 2**20),
        cost_estimate=pl.CostEstimate(flops=4 * total * n * weights[0].shape[0] * width, bytes_accessed=10**6, transcendentals=0),
        name="project_norm",
    )(places, *bases, x, gain, *weights, *residuals)


def up_kernel(half, n, s_ref, in_ref, edge_ref, t_ref, *refs):
    pieces = refs[:n]
    o_ref, x_ref, w_scr, u_scr, e_scr, sems, sems_x = refs[n:]
    block = pieces[0].shape[0]
    copies = gather_in(pieces, w_scr, [pl.multiple_of(s_ref[i], block) for i in range(n)], sems)
    total = x_ref.shape[0]
    rows = 256 if total % 256 == 0 else total

    def take(i):
        at = pl.ds(pl.multiple_of(i * rows, rows), rows)
        return pltpu.make_async_copy(in_ref.at[at], x_ref.at[at], sems_x.at[i])

    for i in range(total // rows):
        take(i).start()
    for copy in copies:
        copy.wait()
    part = 64
    per, last = rows // part, total // part - 1
    e_scr[...] = (
        jnp.dot(edge_ref[...], w_scr[...], preferred_element_type=F32).astype(BF16).astype(F32)
    )
    row = lax.broadcasted_iota(jnp.int32, (part, 2 * half), 0)

    def multiply(i):
        take(i).wait()
        r = pl.multiple_of(i * rows, rows)
        u_scr[pl.ds(r, rows), :] = jnp.dot(
            x_ref[pl.ds(r, rows), :], w_scr[...], preferred_element_type=F32
        ).astype(BF16)

    def mix(i):
        r = pl.multiple_of(i * part, part)
        cur = u_scr[pl.ds(r, part), :].astype(F32)
        up_at = pl.multiple_of(jnp.maximum(r - 16, 0), 16)
        down_at = pl.multiple_of(jnp.minimum(r + part, total - 16), 16)
        above = u_scr[pl.ds(up_at, 16), :].astype(F32)[15:16]
        below = u_scr[pl.ds(down_at, 16), :].astype(F32)[0:1]
        above = jnp.where(i == 0, e_scr[0:1, :], above)
        below = jnp.where(i == last, e_scr[1:2, :], below)
        before = jnp.where(row == 0, above, pltpu.roll(cur, 1, 0))
        after = jnp.where(row == part - 1, below, pltpu.roll(cur, part - 1, 0))
        smooth = t_ref[0:1, :] * before + t_ref[1:2, :] * cur + t_ref[2:3, :] * after
        gate = smooth[:, :half]
        o_ref[pl.ds(r, part), :] = (gate / (1.0 + jnp.exp(-gate)) * smooth[:, half:]).astype(BF16)

    multiply(0)
    if total // rows > 1:
        multiply(1)
        for j in range(per - 1):
            mix(j)

    def step(i, c):
        multiply(i)
        for j in range(per):
            mix((i - 1) * per - 1 + j)
        return c

    lax.fori_loop(2, total // rows, step, 0)

    def rest(i, c):
        mix(i)
        return c

    lax.fori_loop(max(total // rows - 1, 0) * per - (1 if total // rows > 1 else 0), last + 1, rest, 0)


def up_and_mix(places, normed, edge, taps, pieces):
    total, width = normed.shape
    columns = pieces[0].shape[1]
    return pl.pallas_call(
        functools.partial(up_kernel, columns // 2, len(pieces)),
        out_shape=jax.ShapeDtypeStruct((total, columns // 2), BF16),
        in_specs=[SMEM_SPEC, HBM_SPEC] + [VMEM_SPEC] * 2 + [HBM_SPEC] * len(pieces),
        out_specs=VMEM_SPEC,
        scratch_shapes=[
            pltpu.VMEM((total, width), BF16),
            pltpu.VMEM((width, columns), BF16),
            pltpu.VMEM((total, columns), BF16),
            pltpu.VMEM((16, columns), F32),
            pltpu.SemaphoreType.DMA((len(pieces),)),
            pltpu.SemaphoreType.DMA((total // (256 if total % 256 == 0 else total),)),
        ],
        compiler_params=pltpu.CompilerParams(vmem_limit_bytes=60 * 2**20),
        cost_estimate=pl.CostEstimate(flops=2 * total * width * columns, bytes_accessed=10**6, transcendentals=0),
        name="up_and_mix",
    )(places, normed, edge, taps, *pieces)


def down_kernel(n, s_ref, h_ref, *refs):
    pieces = refs[:n]
    keep_ref, send_ref, d_scr, sems = refs[n:]
    block = pieces[0].shape[0]
    copies = gather_in(pieces, d_scr, [pl.multiple_of(s_ref[i], block) for i in range(n)], sems)
    for copy in copies:
        copy.wait()
    far, _, tok, width = keep_ref.shape
    side = s_ref[n]
    rows = tok // 2 if tok % 32 == 0 else tok
    steps = tok // rows

    def multiply(i, c):
        rel = i // steps
        r = pl.multiple_of((i - rel * steps) * rows, rows)
        own = jnp.where(rel == 0, side, 1 - side)
        h = h_ref[pl.ds(pl.multiple_of(own * tok + r, rows), rows), :]
        for o in range(2 * far):
            out = lax.dot_general(
                h,
                d_scr[o * width : (o + 1) * width, :],
                (((1,), (1,)), ((), ())),
                preferred_element_type=F32,
            ).astype(BF16)
            ref = keep_ref if o < far else send_ref
            ref[o % far, rel, pl.ds(r, rows), :] = out
        return c

    lax.fori_loop(0, 2 * steps, multiply, 0)


def down_terms(places, hidden, pieces, tp_size, tok, width):
    shape = jax.ShapeDtypeStruct((tp_size // 2, 2, tok, width), BF16)
    return pl.pallas_call(
        functools.partial(down_kernel, len(pieces)),
        out_shape=(shape, shape),
        in_specs=[SMEM_SPEC, VMEM_SPEC] + [HBM_SPEC] * len(pieces),
        out_specs=(VMEM_SPEC, VMEM_SPEC),
        scratch_shapes=[
            pltpu.VMEM((tp_size * width, hidden.shape[1]), BF16),
            pltpu.SemaphoreType.DMA((len(pieces),)),
        ],
        compiler_params=pltpu.CompilerParams(vmem_limit_bytes=18 * 2**20),
        cost_estimate=pl.CostEstimate(flops=2 * hidden.size * tp_size * width, bytes_accessed=10**6, transcendentals=0),
        name="down_terms",
    )(places, hidden, *pieces)


def per_device(
    sp_size,
    tp_size,
    residual,
    query_wide,
    query_narrow,
    latent,
    rope_key,
    latent_gain,
    expand_wide,
    expand_narrow,
    out_wide,
    out_narrow,
    norm_gain,
    up_gate,
    up_value,
    down_weight,
    conv_taps,
):
    ring = sp_size // 2
    me = lax.axis_index("sp")
    tp = lax.axis_index("tp")
    side = lax.rem(me, 2)
    core = lax.rem(tp, 2)
    tok_rows = residual.shape[0]
    positions = (me * tok_rows + lax.iota(jnp.int32, tok_rows)).astype(jnp.float32)

    def mate(a):
        return lax.ppermute(a, "sp", [(i, i ^ 1) for i in range(sp_size)])

    def along(a, k):
        return lax.ppermute(a, "sp", [(i, (i + 2 * k) % sp_size) for i in range(sp_size)])

    def across(a, bit):
        return lax.ppermute(a, "tp", [(i, i ^ bit) for i in range(tp_size)])

    far_bits = []
    bit = 2
    while bit < tp_size:
        far_bits.append(bit)
        bit *= 2
    tp_order = [0]
    for bit in far_bits + [1]:
        tp_order = tp_order + [p ^ bit for p in tp_order]

    def over_tp(a, axis):
        for bit in far_bits + [1]:
            a = jnp.concatenate([a, across(a, bit)], axis=axis)
        return a

    def spread_tp(a):
        blocks = [a]
        for bit in far_bits + [1]:
            blocks = blocks + [across(b, bit) for b in blocks]
        return blocks

    def paired(own, other):
        return jnp.where(side == 0, jnp.concatenate([own, other]), jnp.concatenate([other, own]))

    latent_float = latent.astype(F32)
    normed_latent = (
        latent_float
        * lax.rsqrt(jnp.mean(latent_float * latent_float, axis=-1, keepdims=True) + epsilon)
        * latent_gain
    ).astype(BF16)
    cosine, sine = angles_of(positions)
    rope_turned = rotate(rope_key, cosine, sine)
    packed = jnp.concatenate([normed_latent, rope_turned, rope_turned], axis=1)
    shares = [bit for bit in (2, 1) if bit < tp_size]
    split_rows = tok_rows // (2 ** len(shares))
    mine = lax.dynamic_slice_in_dim(
        packed, lax.rem(tp, 2 ** len(shares)) * split_rows, split_rows, axis=0
    )
    hops = []
    for _ in range(1, ring):
        hops.append(along(hops[-1] if hops else mine, 1))
    sides = [mate(h) for h in [mine] + hops]
    pieces = [packed]
    for remote in hops + sides:
        group = [remote]
        for bit in shares:
            group = group + [across(g, bit) for g in group]
        pieces = pieces + group

    units = up_gate.shape[1]
    half = units // 2

    def split(a, b):
        low, high = (x[:, :half] for x in (a, b)), (x[:, half:] for x in (a, b))
        low, high = jnp.concatenate(list(low), axis=1), jnp.concatenate(list(high), axis=1)
        return jnp.where(side == 0, low, high), jnp.where(side == 0, high, low)

    up_keep, up_give = split(up_gate, up_value)
    down_keep = jnp.where(side == 0, down_weight[:, :half], down_weight[:, half:])
    down_give = jnp.where(side == 0, down_weight[:, half:], down_weight[:, :half])
    up_a, up_b = [up_keep], [mate(up_give)]
    down_a, down_b = [down_keep], [mate(down_give)]
    for _ in range(1, ring):
        up_a.append(along(up_a[-1], 1))
        up_b.append(along(up_b[-1], 1))
        down_a.append(along(down_a[-1], 1))
        down_b.append(along(down_b[-1], 1))

    outs_w = spread_tp(out_wide)
    outs_n = spread_tp(out_narrow)
    own_width = residual.shape[1]
    pair_residual = paired(residual, mate(residual))
    residuals = spread_tp(pair_residual)
    gains = over_tp(norm_gain[None, :], 1)
    full_gain = jnp.zeros((1, own_width * tp_size), F32)
    lanes_at = []
    for p, q in enumerate(tp_order):
        at = jnp.bitwise_xor(tp, q) * own_width
        lanes_at.append(at)
        piece = slice(p * own_width, (p + 1) * own_width)
        full_gain = lax.dynamic_update_slice_in_dim(full_gain, gains[:, piece], at, axis=1)

    wide_heads = query_wide.shape[1] // (NOPE_W + ROPE)
    narrow_heads = query_narrow.shape[1] // (NOPE_N + ROPE)
    ones, zeros = jnp.ones_like(cosine), jnp.zeros_like(cosine)
    tables_w = (
        jnp.concatenate([cosine, cosine, zeros, zeros], axis=1),
        jnp.concatenate([-sine, sine, zeros, zeros], axis=1),
    )
    tables_n = (
        jnp.concatenate([ones, ones, cosine, cosine], axis=1),
        jnp.concatenate([zeros, zeros, -sine, sine], axis=1),
    )
    heads_w, keys = attend(
        query_wide, tables_w, expand_wide, pieces, wide_heads, True, False,
        (NOPE_W + ROPE) ** (-0.5), passes=True,
    )
    columns = NOPE_N + VAL_N
    heads_n = []
    for h in range(narrow_heads):
        at = slice(h * columns, (h + 1) * columns)
        out = attend(
            query_narrow[:, at], tables_n, expand_narrow[:, at], [keys], 1, False, h % 2 == 1,
            (NOPE_N + ROPE) ** (-0.5),
        )
        if h % 2:
            heads_n[-1] = heads_n[-1] + out
        else:
            heads_n.append(out)
    heads_n = heads_n[0] if len(heads_n) == 1 else jnp.concatenate(heads_n, axis=1)
    heads_n = heads_n[:, : narrow_heads * VAL_N]
    full_w = over_tp(paired(heads_w, mate(heads_w)), 1)
    full_n = over_tp(paired(heads_n, mate(heads_n)), 1)
    lanes_at = jnp.stack(lanes_at + [tp * own_width, side]).astype(jnp.int32)
    bases = []
    for i in range(2):
        bases.append(project_base([full_w], outs_w, i * tok_rows, tok_rows))
    attended, normed, rims = project_norm(lanes_at, bases, full_n, full_gain, outs_n, residuals)

    up_line = [(i, i + 2) for i in range(sp_size - 2)]
    low = lax.ppermute(rims[31:], "sp", up_line)
    high = lax.ppermute(rims[:1], "sp", [(b, a) for a, b in up_line])
    edge = jnp.concatenate([low, high, jnp.zeros((14, normed.shape[1]), BF16)], axis=0)
    block = up_gate.shape[0]
    position = me // 2
    starts, blocks = [], []
    for k in range(ring):
        source = lax.rem(position - k + ring, ring) * 2
        for s in (source + side, source + 1 - side):
            at = s * block
            starts.append(at)
            rel = jnp.bitwise_xor(at // own_width, tp)
            order = lax.rem(rel, 2) * (tp_size // 2) + rel // 2
            blocks.append(order * own_width + lax.rem(at, own_width))
    up_pieces = [p for k in range(ring) for p in (up_a[k], up_b[k])]
    down_pieces = [p for k in range(ring) for p in (down_a[k], down_b[k])]
    taps = jnp.where(side == 0, conv_taps[:, :, :half], conv_taps[:, :, half:]).reshape(3, 2 * half)
    taps = jnp.pad(taps, ((0, 5), (0, 0)))
    hidden = up_and_mix(jnp.stack(starts).astype(jnp.int32), normed, edge, taps, up_pieces)
    kept, sent = down_terms(
        jnp.stack(blocks + [side]).astype(jnp.int32), hidden, down_pieces, tp_size, tok_rows, own_width
    )

    def add(a, b):
        return (a.astype(F32) + b.astype(F32)).astype(BF16)

    terms = add(kept, across(sent, 1))
    for bit in far_bits[:0:-1]:
        n = terms.shape[0] // 2
        terms = add(terms[:n], across(terms[n:], bit))
    cut = tok_rows // 2
    first, second = terms[:, :, :cut], terms[:, :, cut:]
    got_x = across(second[1], 2)
    got_y = mate(first[:, 1])
    more_x = across(add(first[1, 0], got_y[1]), 2)
    more_y = mate(add(second[0, 1], got_x[1]))
    own = attended.astype(F32)
    out_first = own[:cut] + (first[0, 0].astype(F32) + got_y[0].astype(F32) + more_x.astype(F32))
    out_second = own[cut:] + (second[0, 0].astype(F32) + got_x[0].astype(F32) + more_y.astype(F32))
    return jnp.concatenate([out_first, out_second], axis=0).astype(BF16)


def solution(mesh):
    in_specs = (
        P("sp", "tp"),
        P("sp", "tp"),
        P("sp", "tp"),
        P("sp", None),
        P("sp", None),
        P(),
        P(None, "tp"),
        P(None, "tp"),
        P("tp", None),
        P("tp", None),
        P("tp"),
        P("sp", "tp"),
        P("sp", "tp"),
        P("sp", "tp"),
        P(None, None, "tp"),
    )
    out_specs = P("sp", "tp")

    def body(*args):
        return per_device(mesh.shape["sp"], mesh.shape["tp"], *args)

    return jax.shard_map(body, mesh=mesh, in_specs=in_specs, out_specs=out_specs, check_vma=False)
```

profile of v0, /device:TPU:0, one launch (start us, length us, event | category | flops | bytes accessed | tf_op | source)
XLA Modules:
  0.0 356.4 jit_solution(12253483528723874566)
XLA Ops:
  2.7 1.5 fusion.15
  4.3 1.9 concatenate.71.refs_4_
  6.3 3.1 collective-permute-start
  9.4 1.5 collective-permute-start.12
  10.9 5.6 %collective-permute-done.refs_5_ = bf16[160,640]{1,0:T(8,128)(2,1)S(1)} collective-permute-done((bf16[160,640]{1,0:T(8,128)(2,1)S(1)}, bf16[160,640]{1,0:T(8,128)(2,1)S(1)}, u32[]{:S(2)}, u32[]{:S(2)}) %collective-permute-start) | collective-permute-done | bytes 204832 | tf_op jit(solution)/shard_map/ppermute | solution.py:539
  16.5 1.6 collective-permute-start.37
  18.0 1.5 collective-permute-start.16
  20.1 1.6 collective-permute-start.13
  21.7 2.8 collective-permute-done.4.refs_9_
  24.5 1.9 fusion.16
  27.9 1.5 collective-permute-start.5
  31.0 1.7 broadcast_select_fusion
  32.7 3.0 collective-permute-done.8.refs_13_
  37.8 1.7 collective-permute-done.17.refs_22_
  39.4 1.5 collective-permute-start.9
  40.9 1.7 pad_maximum_fusion.10
  44.0 1.7 collective-permute-done.9.refs_14_
  45.7 2.3 collective-permute-start.25
  48.2 2.6 collective-permute-done.21.refs_26_
  51.8 2.8 collective-permute-done.25.refs_30_
  57.5 1.6 collective-permute-start.55
  59.8 26.8 %shard_map.145 = (bf16[640,256]{1,0:T(8,128)(2,1)}, bf16[5120,640]{1,0:T(8,128)(2,1)}) custom-call(bf16[640,384]{1,0:T(8,128)(2,1)} %refs_0_.1, f32[640,128]{1,0:T(8,128)} %get-tuple-element.37.refs_1_, f32[640,128]{1,0:T(8,128)} %get-tuple-element.26.refs_2_, bf16[512,512]{1,0:T(8,128)(2,1)} %refs_3_.1, bf16[640,640]{1,0:T(8,128)(2,1)} %copy-done.18, ...), custom_call_target="tpu_custom_call" | custom-call | flops 5033164800 | bytes 5242880 | tf_op jit(solution)/shard_map/pallas_call | solution.py:230
  88.0 1.5 collective-permute-start.48
  89.5 14.7 %shard_map.146 = bf16[640,128]{1,0:T(8,128)(2,1)} custom-call(bf16[640,128]{1,0:T(8,128)(2,1)} %get-tuple-element.36.refs_0_, f32[640,128]{1,0:T(8,128)} %get-tuple-element.38.refs_1_, f32[640,128]{1,0:T(8,128)} %get-tuple-element.25.refs_2_, bf16[512,128]{1,0:T(8,128)(2,1)} %get-tuple-element.40.refs_3_, bf16[5120,640]{1,0:T(8,128)(2,1)} %get-tuple-element.13.refs_4_), custom_call_target="tpu_custom_call" | custom-call | flops 1677721600 | bytes 5242880 | tf_op jit(solution)/shard_map/pallas_call | solution.py:230
  106.7 1.5 collective-permute-start.29
  108.2 14.5 %shard_map.147 = bf16[640,128]{1,0:T(8,128)(2,1)} custom-call(bf16[640,128]{1,0:T(8,128)(2,1)} %get-tuple-element.35.refs_0_, f32[640,128]{1,0:T(8,128)} %get-tuple-element.38.refs_1_, f32[640,128]{1,0:T(8,128)} %get-tuple-element.25.refs_2_, bf16[512,128]{1,0:T(8,128)(2,1)} %get-tuple-element.39.refs_3_, bf16[5120,640]{1,0:T(8,128)(2,1)} %get-tuple-element.13.refs_4_), custom_call_target="tpu_custom_call" | custom-call | flops 1677721600 | bytes 5242880 | tf_op jit(solution)/shard_map/pallas_call | solution.py:230
  126.0 2.1 maximum_select_fusion.refs_8_
  128.3 2.2 collective-permute-done.34
  132.7 3.2 collective-permute-start.57
  135.9 2.4 pad_maximum_fusion.1
  138.3 46.2 %collective-permute-done.35 = bf16[1280,128]{1,0:T(8,128)(2,1)S(1)} collective-permute-done((bf16[1280,128]{1,0:T(8,128)(2,1)S(1)}, bf16[1280,128]{1,0:T(8,128)(2,1)S(1)}, u32[]{:S(2)}, u32[]{:S(2)}) %collective-permute-start.35) | collective-permute-done | bytes 327712 | tf_op jit(solution)/shard_map/ppermute | solution.py:542
  187.3 2.7 collective-permute-start.50
  192.0 15.9 %collective-permute-done.50.refs_3_ = bf16[256,1408]{1,0:T(8,128)(2,1)S(1)} collective-permute-done((bf16[256,1408]{1,0:T(8,128)(2,1)}, bf16[256,1408]{1,0:T(8,128)(2,1)S(1)}, u32[]{:S(2)}, u32[]{:S(2)}) %collective-permute-start.50) | collective-permute-done | bytes 720928 | tf_op jit(solution)/shard_map/ppermute | solution.py:539
  209.2 2.0 pad_maximum_fusion.refs_0_
  211.2 5.3 %project_base.3.refs_1_ = bf16[640,2048]{1,0:T(8,128)(2,1)S(1)} custom-call(bf16[1280,1024]{1,0:T(8,128)(2,1)S(1)} %pad_maximum_fusion.refs_0_, bf16[256,2048]{1,0:T(8,128)(2,1)} %refs_1_.3, bf16[256,2048]{1,0:T(8,128)(2,1)} %collective-permute-done.31.refs_2_, bf16[256,2048]{1,0:T(8,128)(2,1)} %collective-permute-done.32.refs_3_, ...), custom_call_target="tpu_custom_call" | custom-call | flops 2684354560 | bytes 1000000 | tf_op jit(solution)/shard_map/project_base/pallas_call | solution.py:279
  216.5 5.4 %project_base.2.refs_0_ = bf16[640,2048]{1,0:T(8,128)(2,1)S(1)} custom-call(bf16[1280,1024]{1,0:T(8,128)(2,1)S(1)} %pad_maximum_fusion.refs_0_, bf16[256,2048]{1,0:T(8,128)(2,1)} %refs_1_.3, bf16[256,2048]{1,0:T(8,128)(2,1)} %collective-permute-done.31.refs_2_, bf16[256,2048]{1,0:T(8,128)(2,1)} %collective-permute-done.32.refs_3_, ...), custom_call_target="tpu_custom_call" | custom-call | flops 2684354560 | bytes 1000000 | tf_op jit(solution)/shard_map/project_base/pallas_call | solution.py:279
  222.6 6.5 %collective-permute-done.51.refs_4_ = bf16[256,1408]{1,0:T(8,128)(2,1)} collective-permute-done((bf16[256,1408]{1,0:T(8,128)(2,1)}, bf16[256,1408]{1,0:T(8,128)(2,1)}, u32[]{:S(2)}, u32[]{:S(2)}) %collective-permute-start.51) | collective-permute-done | bytes 720928 | tf_op jit(solution)/shard_map/ppermute | solution.py:539
  229.1 15.4 %collective-permute-done.52.refs_5_ = bf16[256,1408]{1,0:T(8,128)(2,1)} collective-permute-done((bf16[256,1408]{1,0:T(8,128)(2,1)S(1)}, bf16[256,1408]{1,0:T(8,128)(2,1)}, u32[]{:S(2)}, u32[]{:S(2)}) %collective-permute-start.52) | collective-permute-done | bytes 720928 | tf_op jit(solution)/shard_map/ppermute | solution.py:539
  244.6 9.5 %project_norm.1 = (bf16[640,512]{1,0:T(8,128)(2,1)S(1)}, bf16[1280,2048]{1,0:T(8,128)(2,1)S(1)}, bf16[32,2048]{1,0:T(8,128)(2,1)S(1)}) custom-call(s32[6]{0:T(128)S(1)} %stack.79.s_ref, bf16[640,2048]{1,0:T(8,128)(2,1)S(1)} %project_base.2.refs_0_, bf16[640,2048]{1,0:T(8,128)(2,1)S(1)} %project_base.3.refs_1_, ...), custom_call_target="tpu_custom_call" | custom-call | flops 2684354560 | bytes 1000000 | tf_op jit(solution)/shard_map/project_norm/pallas_call | solution.py:348
  254.1 2.3 copy-done.8
  262.7 26.2 %collective-permute-done.46 = bf16[1,2048]{1,0:T(2,128)(2,1)S(1)} collective-permute-done((bf16[1,2048]{1,0:T(2,128)(2,1)S(1)}, bf16[1,2048]{1,0:T(2,128)(2,1)S(1)}, u32[]{:S(2)}, u32[]{:S(2)}) %collective-permute-start.46) | collective-permute-done | bytes 4128 | tf_op jit(solution)/shard_map/ppermute | solution.py:663
  288.9 2.5 collective-permute-start.61
  293.0 20.6 %up_and_mix.1.h_ref = bf16[1280,704]{1,0:T(8,128)(2,1)} custom-call(s32[8]{0:T(128)} %stack.97.s_ref, bf16[1280,2048]{1,0:T(8,128)(2,1)} %copy-done.8, bf16[16,2048]{1,0:T(8,128)(2,1)} %maximum_maximum_fusion.edge_ref, f32[8,1408]{1,0:T(8,128)} %pad.4.t_ref, bf16[256,1408]{1,0:T(8,128)(2,1)} %get-tuple-element.24.refs_0_, ...), custom_call_target="tpu_custom_call" | custom-call | flops 7381975040 | bytes 1000000 | tf_op jit(solution)/shard_map/up_and_mix/pallas_call | solution.py:441
  313.7 1.5 copy-done.14
  315.2 7.3 %down_terms.1 = (bf16[2,2,640,512]{3,2,1,0:T(8,128)(2,1)S(1)}, bf16[2,2,640,512]{3,2,1,0:T(8,128)(2,1)S(1)}) custom-call(s32[9]{0:T(128)S(1)} %stack.88.s_ref, bf16[1280,704]{1,0:T(8,128)(2,1)S(1)} %copy-done.14, bf16[256,704]{1,0:T(8,128)(2,1)S(1)} %copy-done.7, bf16[256,704]{1,0:T(8,128)(2,1)S(1)} %copy-done.10, bf16[256,704]{1,0:T(8,128)(2,1)S(1)} %copy-done.13, ...), custom_call_target="tpu_custom_call" | custom-call | flops 3690987520 | bytes 1000000 | tf_op jit(solution)/shard_map/down_terms/pallas_call | solution.py:493
  322.6 4.9 %collective-permute-done.62 = bf16[2,2,640,512]{3,2,1,0:T(8,128)(2,1)S(1)} collective-permute-done((bf16[2,2,640,512]{3,2,1,0:T(8,128)(2,1)S(1)}, bf16[2,2,640,512]{3,2,1,0:T(8,128)(2,1)S(1)}, u32[]{:S(2)}, u32[]{:S(2)}) %collective-permute-start.62) | collective-permute-done | bytes 2621472 | tf_op jit(solution)/shard_map/ppermute | solution.py:542
  330.1 15.2 %collective-permute-done.63 = bf16[2,320,512]{2,1,0:T(8,128)(2,1)S(1)} collective-permute-done((bf16[2,320,512]{2,1,0:T(8,128)(2,1)S(1)}, bf16[2,320,512]{2,1,0:T(8,128)(2,1)S(1)}, u32[]{:S(2)}, u32[]{:S(2)}) %collective-permute-start.63) | collective-permute-done | bytes 655392 | tf_op jit(solution)/shard_map/ppermute | solution.py:536
  348.0 6.5 %collective-permute-done.64 = bf16[320,512]{1,0:T(8,128)(2,1)S(1)} collective-permute-done((bf16[320,512]{1,0:T(8,128)(2,1)S(1)}, bf16[320,512]{1,0:T(8,128)(2,1)S(1)}, u32[]{:S(2)}, u32[]{:S(2)}) %collective-permute-start.64) | collective-permute-done | bytes 327712 | tf_op jit(solution)/shard_map/ppermute | solution.py:542
  (258 shorter events, 45.1 us)
Async XLA Ops:
  6.3 10.2 %collective-permute-start = (bf16[160,640]{1,0:T(8,128)(2,1)S(1)}, bf16[160,640]{1,0:T(8,128)(2,1)S(1)}, u32[]{:S(2)}, u32[]{:S(2)}) collective-permute-start(bf16[160,640]{1,0:T(8,128)(2,1)S(1)} %constant_dynamic-slice_fusion), channel_id=1, source_target_pairs={{0,8},{4,12},{8,16},{12,20},{16,24},{20,28},{24,0},{28,4},{1,9},{5... | collective-permute-start | bytes 614408 | tf_op jit(solution)/shard_map/ppermute | solution.py:539
  9.4 10.8 %collective-permute-start.12 = (bf16[160,640]{1,0:T(8,128)(2,1)S(1)}, bf16[160,640]{1,0:T(8,128)(2,1)S(1)}, u32[]{:S(2)}, u32[]{:S(2)}) collective-permute-start(bf16[160,640]{1,0:T(8,128)(2,1)S(1)} %constant_dynamic-slice_fusion), channel_id=1, source_target_pairs={{0,4},{4,0},{8,12},{12,8},{16,20},{20,16},{24,28},{28,24},{1,5},{5... | collective-permute-start | bytes 614408 | tf_op jit(solution)/shard_map/ppermute | solution.py:536
  16.5 8.0 %collective-permute-start.4 = (bf16[160,640]{1,0:T(8,128)(2,1)S(1)}, bf16[160,640]{1,0:T(8,128)(2,1)S(1)}, u32[]{:S(2)}, u32[]{:S(2)}) collective-permute-start(bf16[160,640]{1,0:T(8,128)(2,1)S(1)} %collective-permute-done.refs_5_), channel_id=1, source_target_pairs={{0,8},{4,12},{8,16},{12,20},{16,24},{20,28},{24,0},{28,4},{1,9},{5... | collective-permute-start | bytes 614408 | tf_op jit(solution)/shard_map/ppermute | solution.py:539
  18.0 8.4 %collective-permute-start.16 = (bf16[160,640]{1,0:T(8,128)(2,1)S(1)}, bf16[160,640]{1,0:T(8,128)(2,1)S(1)}, u32[]{:S(2)}, u32[]{:S(2)}) collective-permute-start(bf16[160,640]{1,0:T(8,128)(2,1)S(1)} %collective-permute-done.refs_5_), channel_id=1, source_target_pairs={{0,4},{4,0},{8,12},{12,8},{16,20},{20,16},{24,28},{28,24},{1,5},{5... | collective-permute-start | bytes 614408 | tf_op jit(solution)/shard_map/ppermute | solution.py:536
  20.1 9.6 %collective-permute-start.13 = (bf16[160,640]{1,0:T(8,128)(2,1)S(1)}, bf16[160,640]{1,0:T(8,128)(2,1)S(1)}, u32[]{:S(2)}, u32[]{:S(2)}) collective-permute-start(bf16[160,640]{1,0:T(8,128)(2,1)S(1)} %collective-permute-done.12.refs_17_), channel_id=1, source_target_pairs={{0,2},{1,3},{2,0},{3,1},{4,6},{5,7},{6,4},{7,5},{8,10},{9,11},{10,... | collective-permute-start | bytes 614408 | tf_op jit(solution)/shard_map/ppermute | solution.py:542
  26.4 9.3 %collective-permute-start.8 = (bf16[160,640]{1,0:T(8,128)(2,1)S(1)}, bf16[160,640]{1,0:T(8,128)(2,1)S(1)}, u32[]{:S(2)}, u32[]{:S(2)}) collective-permute-start(bf16[160,640]{1,0:T(8,128)(2,1)S(1)} %collective-permute-done.4.refs_9_), channel_id=1, source_target_pairs={{0,8},{4,12},{8,16},{12,20},{16,24},{20,28},{24,0},{28,4},{1,9},{5... | collective-permute-start | bytes 614408 | tf_op jit(solution)/shard_map/ppermute | solution.py:539
  27.4 8.3 %collective-permute-start.20 = (bf16[160,640]{1,0:T(8,128)(2,1)S(1)}, bf16[160,640]{1,0:T(8,128)(2,1)S(1)}, u32[]{:S(2)}, u32[]{:S(2)}) collective-permute-start(bf16[160,640]{1,0:T(8,128)(2,1)S(1)} %collective-permute-done.4.refs_9_), channel_id=1, source_target_pairs={{0,4},{4,0},{8,12},{12,8},{16,20},{20,16},{24,28},{28,24},{1,5},{5... | collective-permute-start | bytes 614408 | tf_op jit(solution)/shard_map/ppermute | solution.py:536
  27.9 8.4 %collective-permute-start.5 = (bf16[160,640]{1,0:T(8,128)(2,1)S(1)}, bf16[160,640]{1,0:T(8,128)(2,1)S(1)}, u32[]{:S(2)}, u32[]{:S(2)}) collective-permute-start(bf16[160,640]{1,0:T(8,128)(2,1)S(1)} %collective-permute-done.4.refs_9_), channel_id=1, source_target_pairs={{0,2},{1,3},{2,0},{3,1},{4,6},{5,7},{6,4},{7,5},{8,10},{9,11},{10,... | collective-permute-start | bytes 614408 | tf_op jit(solution)/shard_map/ppermute | solution.py:542
  30.5 9.0 %collective-permute-start.17 = (bf16[160,640]{1,0:T(8,128)(2,1)S(1)}, bf16[160,640]{1,0:T(8,128)(2,1)S(1)}, u32[]{:S(2)}, u32[]{:S(2)}) collective-permute-start(bf16[160,640]{1,0:T(8,128)(2,1)S(1)} %collective-permute-done.16.refs_21_), channel_id=1, source_target_pairs={{0,2},{1,3},{2,0},{3,1},{4,6},{5,7},{6,4},{7,5},{8,10},{9,11},{10,... | collective-permute-start | bytes 614408 | tf_op jit(solution)/shard_map/ppermute | solution.py:542
  42.7 8.1 %collective-permute-start.10 = (bf16[160,640]{1,0:T(8,128)(2,1)S(1)}, bf16[160,640]{1,0:T(8,128)(2,1)S(1)}, u32[]{:S(2)}, u32[]{:S(2)}) collective-permute-start(bf16[160,640]{1,0:T(8,128)(2,1)S(1)} %collective-permute-done.8.refs_13_), channel_id=1, source_target_pairs={{0,1},{1,0},{2,3},{3,2},{4,5},{5,4},{6,7},{7,6},{8,9},{9,8},{10,11... | collective-permute-start | bytes 614408 | tf_op jit(solution)/shard_map/ppermute | solution.py:542
  42.8 8.0 %collective-permute-start.21 = (bf16[160,640]{1,0:T(8,128)(2,1)S(1)}, bf16[160,640]{1,0:T(8,128)(2,1)S(1)}, u32[]{:S(2)}, u32[]{:S(2)}) collective-permute-start(bf16[160,640]{1,0:T(8,128)(2,1)S(1)} %collective-permute-done.20.refs_25_), channel_id=1, source_target_pairs={{0,2},{1,3},{2,0},{3,1},{4,6},{5,7},{6,4},{7,5},{8,10},{9,11},{10,... | collective-permute-start | bytes 614408 | tf_op jit(solution)/shard_map/ppermute | solution.py:542
  43.4 7.9 %collective-permute-start.22 = (bf16[160,640]{1,0:T(8,128)(2,1)S(1)}, bf16[160,640]{1,0:T(8,128)(2,1)S(1)}, u32[]{:S(2)}, u32[]{:S(2)}) collective-permute-start(bf16[160,640]{1,0:T(8,128)(2,1)S(1)} %collective-permute-done.20.refs_25_), channel_id=1, source_target_pairs={{0,1},{1,0},{2,3},{3,2},{4,5},{5,4},{6,7},{7,6},{8,9},{9,8},{10,11... | collective-permute-start | bytes 614408 | tf_op jit(solution)/shard_map/ppermute | solution.py:542
  45.7 8.9 %collective-permute-start.25 = (bf16[160,640]{1,0:T(8,128)(2,1)S(1)}, bf16[160,640]{1,0:T(8,128)(2,1)S(1)}, u32[]{:S(2)}, u32[]{:S(2)}) collective-permute-start(bf16[160,640]{1,0:T(8,128)(2,1)S(1)} %collective-permute-done.24.refs_29_), channel_id=1, source_target_pairs={{0,2},{1,3},{2,0},{3,1},{4,6},{5,7},{6,4},{7,5},{8,10},{9,11},{10,... | collective-permute-start | bytes 614408 | tf_op jit(solution)/shard_map/ppermute | solution.py:542
  55.5 69.5 %collective-permute-start.42 = (bf16[640,512]{1,0:T(8,128)(2,1)}, bf16[640,512]{1,0:T(8,128)(2,1)}, u32[]{:S(2)}, u32[]{:S(2)}) collective-permute-start(bf16[640,512]{1,0:T(8,128)(2,1)} %param.15), channel_id=1, source_target_pairs={{0,4},{4,0},{8,12},{12,8},{16,20},{20,16},{24,28},{28,24},{1,5},{5... | collective-permute-start | bytes 1966088 | tf_op jit(solution)/shard_map/ppermute | solution.py:536
  56.1 50.6 %collective-permute-start.39 = (bf16[128,2048]{1,0:T(8,128)(2,1)S(1)}, bf16[128,2048]{1,0:T(8,128)(2,1)S(1)}, u32[]{:S(2)}, u32[]{:S(2)}) collective-permute-start(bf16[128,2048]{1,0:T(8,128)(2,1)S(1)} %copy-done), channel_id=1, source_target_pairs={{0,2},{1,3},{2,0},{3,1},{4,6},{5,7},{6,4},{7,5},{8,10},{9,11},{10,... | collective-permute-start | bytes 1572872 | tf_op jit(solution)/shard_map/ppermute | solution.py:542
  57.5 30.5 %collective-permute-start.55 = (bf16[256,704]{1,0:T(8,128)(2,1)S(1)}, bf16[256,704]{1,0:T(8,128)(2,1)S(1)}, u32[]{:S(2)}, u32[]{:S(2)}) collective-permute-start(bf16[256,704]{1,0:T(8,128)(2,1)S(1)} %get-tuple-element.27), channel_id=1, source_target_pairs={{0,4},{4,0},{8,12},{12,8},{16,20},{20,16},{24,28},{28,24},{1,5},{5... | collective-permute-start | bytes 1081352 | tf_op jit(solution)/shard_map/ppermute | solution.py:536
  59.1 28.9 %collective-permute-start.56 = (bf16[256,704]{1,0:T(8,128)(2,1)S(1)}, bf16[256,704]{1,0:T(8,128)(2,1)S(1)}, u32[]{:S(2)}, u32[]{:S(2)}) collective-permute-start(bf16[256,704]{1,0:T(8,128)(2,1)S(1)} %get-tuple-element.28.refs_0_), channel_id=1, source_target_pairs={{0,8},{4,12},{8,16},{12,20},{16,24},{20,28},{24,0},{28,4},{1,9},{5... | collective-permute-start | bytes 1081352 | tf_op jit(solution)/shard_map/ppermute | solution.py:539
  59.1 27.5 %collective-permute-start.38 = (f32[1,1024]{1,0:T(1,128)S(1)}, f32[1,1024]{1,0:T(1,128)S(1)}, u32[]{:S(2)}, u32[]{:S(2)}) collective-permute-start(f32[1,1024]{1,0:T(1,128)S(1)} %pad_maximum_fusion.11), channel_id=1, source_target_pairs={{0,1},{1,0},{2,3},{3,2},{4,5},{5,4},{6,7},{7,6},{8,9},{9,8},{10,11... | collective-permute-start | bytes 12296 | tf_op jit(solution)/shard_map/ppermute | solution.py:542
  86.6 17.6 %collective-permute-start.28 = (bf16[640,256]{1,0:T(8,128)(2,1)}, bf16[640,256]{1,0:T(8,128)(2,1)S(1)}, u32[]{:S(2)}, u32[]{:S(2)}) collective-permute-start(bf16[640,256]{1,0:T(8,128)(2,1)} %get-tuple-element.12), channel_id=1, source_target_pairs={{0,4},{4,0},{8,12},{12,8},{16,20},{20,16},{24,28},{28,24},{1,5},{5... | collective-permute-start | bytes 983048 | tf_op jit(solution)/shard_map/ppermute | solution.py:536
  88.0 35.7 %collective-permute-start.40 = (bf16[128,2048]{1,0:T(8,128)(2,1)S(1)}, bf16[128,2048]{1,0:T(8,128)(2,1)S(1)}, u32[]{:S(2)}, u32[]{:S(2)}) collective-permute-start(bf16[128,2048]{1,0:T(8,128)(2,1)S(1)} %copy-done), channel_id=1, source_target_pairs={{0,1},{1,0},{2,3},{3,2},{4,5},{5,4},{6,7},{7,6},{8,9},{9,8},{10,11... | collective-permute-start | bytes 1572872 | tf_op jit(solution)/shard_map/ppermute | solution.py:542
  88.0 40.2 %collective-permute-start.48 = (bf16[256,1408]{1,0:T(8,128)(2,1)S(1)}, bf16[256,1408]{1,0:T(8,128)(2,1)}, u32[]{:S(2)}, u32[]{:S(2)}) collective-permute-start(bf16[256,1408]{1,0:T(8,128)(2,1)S(1)} %copy-done.20), channel_id=1, source_target_pairs={{0,4},{4,0},{8,12},{12,8},{16,20},{20,16},{24,28},{28,24},{1,5},{5... | collective-permute-start | bytes 2162696 | tf_op jit(solution)/shard_map/ppermute | solution.py:536
  104.2 27.9 %collective-permute-start.49 = (bf16[256,1408]{1,0:T(8,128)(2,1)}, bf16[256,1408]{1,0:T(8,128)(2,1)}, u32[]{:S(2)}, u32[]{:S(2)}) collective-permute-start(bf16[256,1408]{1,0:T(8,128)(2,1)} %get-tuple-element.24.refs_0_), channel_id=1, source_target_pairs={{0,8},{4,12},{8,16},{12,20},{16,24},{20,28},{24,0},{28,4},{1,9},{5... | collective-permute-start | bytes 2162696 | tf_op jit(solution)/shard_map/ppermute | solution.py:539
  106.7 26.0 %collective-permute-start.29 = (bf16[1280,256]{1,0:T(8,128)(2,1)}, bf16[1280,256]{1,0:T(8,128)(2,1)}, u32[]{:S(2)}, u32[]{:S(2)}) collective-permute-start(bf16[1280,256]{1,0:T(8,128)(2,1)} %maximum_select_fusion.1), channel_id=1, source_target_pairs={{0,2},{1,3},{2,0},{3,1},{4,6},{5,7},{6,4},{7,5},{8,10},{9,11},{10,... | collective-permute-start | bytes 1966088 | tf_op jit(solution)/shard_map/ppermute | solution.py:542
  124.5 61.0 %collective-permute-start.31 = (bf16[256,2048]{1,0:T(8,128)(2,1)}, bf16[256,2048]{1,0:T(8,128)(2,1)}, u32[]{:S(2)}, u32[]{:S(2)}) collective-permute-start(bf16[256,2048]{1,0:T(8,128)(2,1)} %refs_1_.3), channel_id=1, source_target_pairs={{0,2},{1,3},{2,0},{3,1},{4,6},{5,7},{6,4},{7,5},{8,10},{9,11},{10,... | collective-permute-start | bytes 3145736 | tf_op jit(solution)/shard_map/ppermute | solution.py:542
  128.2 59.2 %collective-permute-start.32 = (bf16[256,2048]{1,0:T(8,128)(2,1)}, bf16[256,2048]{1,0:T(8,128)(2,1)}, u32[]{:S(2)}, u32[]{:S(2)}) collective-permute-start(bf16[256,2048]{1,0:T(8,128)(2,1)} %refs_1_.3), channel_id=1, source_target_pairs={{0,1},{1,0},{2,3},{3,2},{4,5},{5,4},{6,7},{7,6},{8,9},{9,8},{10,11... | collective-permute-start | bytes 3145736 | tf_op jit(solution)/shard_map/ppermute | solution.py:542
  130.5 59.6 %collective-permute-start.43 = (bf16[1280,512]{1,0:T(8,128)(2,1)S(1)}, bf16[1280,512]{1,0:T(8,128)(2,1)S(1)}, u32[]{:S(2)}, u32[]{:S(2)}) collective-permute-start(bf16[1280,512]{1,0:T(8,128)(2,1)S(1)} %maximum_select_fusion.refs_8_), channel_id=1, source_target_pairs={{0,2},{1,3},{2,0},{3,1},{4,6},{5,7},{6,4},{7,5},{8,10},{9,11},{10,... | collective-permute-start | bytes 3932168 | tf_op jit(solution)/shard_map/ppermute | solution.py:542
  132.1 52.4 %collective-permute-start.35 = (bf16[1280,128]{1,0:T(8,128)(2,1)S(1)}, bf16[1280,128]{1,0:T(8,128)(2,1)S(1)}, u32[]{:S(2)}, u32[]{:S(2)}) collective-permute-start(bf16[1280,128]{1,0:T(8,128)(2,1)S(1)} %maximum_select_fusion.2), channel_id=1, source_target_pairs={{0,2},{1,3},{2,0},{3,1},{4,6},{5,7},{6,4},{7,5},{8,10},{9,11},{10,... | collective-permute-start | bytes 983048 | tf_op jit(solution)/shard_map/ppermute | solution.py:542
  132.7 53.2 %collective-permute-start.57 = (bf16[256,704]{1,0:T(8,128)(2,1)S(1)}, bf16[256,704]{1,0:T(8,128)(2,1)}, u32[]{:S(2)}, u32[]{:S(2)}) collective-permute-start(bf16[256,704]{1,0:T(8,128)(2,1)S(1)} %collective-permute-done.55.refs_1_), channel_id=1, source_target_pairs={{0,8},{4,12},{8,16},{12,20},{16,24},{20,28},{24,0},{28,4},{1,9},{5... | collective-permute-start | bytes 1081352 | tf_op jit(solution)/shard_map/ppermute | solution.py:539
  184.5 24.3 %collective-permute-start.30 = (bf16[1280,512]{1,0:T(8,128)(2,1)}, bf16[1280,512]{1,0:T(8,128)(2,1)}, u32[]{:S(2)}, u32[]{:S(2)}) collective-permute-start(bf16[1280,512]{1,0:T(8,128)(2,1)} %pad_maximum_fusion.1), channel_id=1, source_target_pairs={{0,1},{1,0},{2,3},{3,2},{4,5},{5,4},{6,7},{7,6},{8,9},{9,8},{10,11... | collective-permute-start | bytes 3932168 | tf_op jit(solution)/shard_map/ppermute | solution.py:542
  185.5 22.4 %collective-permute-start.33 = (bf16[256,2048]{1,0:T(8,128)(2,1)}, bf16[256,2048]{1,0:T(8,128)(2,1)}, u32[]{:S(2)}, u32[]{:S(2)}) collective-permute-start(bf16[256,2048]{1,0:T(8,128)(2,1)} %collective-permute-done.31.refs_2_), channel_id=1, source_target_pairs={{0,1},{1,0},{2,3},{3,2},{4,5},{5,4},{6,7},{7,6},{8,9},{9,8},{10,11... | collective-permute-start | bytes 3145736 | tf_op jit(solution)/shard_map/ppermute | solution.py:542
  187.3 20.5 %collective-permute-start.50 = (bf16[256,1408]{1,0:T(8,128)(2,1)}, bf16[256,1408]{1,0:T(8,128)(2,1)S(1)}, u32[]{:S(2)}, u32[]{:S(2)}) collective-permute-start(bf16[256,1408]{1,0:T(8,128)(2,1)} %collective-permute-done.48.refs_1_), channel_id=1, source_target_pairs={{0,8},{4,12},{8,16},{12,20},{16,24},{20,28},{24,0},{28,4},{1,9},{5... | collective-permute-start | bytes 2162696 | tf_op jit(solution)/shard_map/ppermute | solution.py:539
  190.0 39.0 %collective-permute-start.44 = (bf16[1280,512]{1,0:T(8,128)(2,1)S(1)}, bf16[1280,512]{1,0:T(8,128)(2,1)S(1)}, u32[]{:S(2)}, u32[]{:S(2)}) collective-permute-start(bf16[1280,512]{1,0:T(8,128)(2,1)S(1)} %maximum_select_fusion.refs_8_), channel_id=1, source_target_pairs={{0,1},{1,0},{2,3},{3,2},{4,5},{5,4},{6,7},{7,6},{8,9},{9,8},{10,11... | collective-permute-start | bytes 3932168 | tf_op jit(solution)/shard_map/ppermute | solution.py:542
  190.3 54.2 %collective-permute-start.45 = (bf16[1280,512]{1,0:T(8,128)(2,1)S(1)}, bf16[1280,512]{1,0:T(8,128)(2,1)S(1)}, u32[]{:S(2)}, u32[]{:S(2)}) collective-permute-start(bf16[1280,512]{1,0:T(8,128)(2,1)S(1)} %collective-permute-done.43.refs_9_), channel_id=1, source_target_pairs={{0,1},{1,0},{2,3},{3,2},{4,5},{5,4},{6,7},{7,6},{8,9},{9,8},{10,11... | collective-permute-start | bytes 3932168 | tf_op jit(solution)/shard_map/ppermute | solution.py:542
  207.9 14.0 %collective-permute-start.41 = (bf16[128,2048]{1,0:T(8,128)(2,1)S(1)}, bf16[128,2048]{1,0:T(8,128)(2,1)S(1)}, u32[]{:S(2)}, u32[]{:S(2)}) collective-permute-start(bf16[128,2048]{1,0:T(8,128)(2,1)S(1)} %collective-permute-done.39.refs_5_), channel_id=1, source_target_pairs={{0,1},{1,0},{2,3},{3,2},{4,5},{5,4},{6,7},{7,6},{8,9},{9,8},{10,11... | collective-permute-start | bytes 1572872 | tf_op jit(solution)/shard_map/ppermute | solution.py:542
  207.9 21.2 %collective-permute-start.51 = (bf16[256,1408]{1,0:T(8,128)(2,1)}, bf16[256,1408]{1,0:T(8,128)(2,1)}, u32[]{:S(2)}, u32[]{:S(2)}) collective-permute-start(bf16[256,1408]{1,0:T(8,128)(2,1)} %collective-permute-done.49.refs_2_), channel_id=1, source_target_pairs={{0,8},{4,12},{8,16},{12,20},{16,24},{20,28},{24,0},{28,4},{1,9},{5... | collective-permute-start | bytes 2162696 | tf_op jit(solution)/shard_map/ppermute | solution.py:539
  208.8 35.7 %collective-permute-start.52 = (bf16[256,1408]{1,0:T(8,128)(2,1)S(1)}, bf16[256,1408]{1,0:T(8,128)(2,1)}, u32[]{:S(2)}, u32[]{:S(2)}) collective-permute-start(bf16[256,1408]{1,0:T(8,128)(2,1)S(1)} %collective-permute-done.50.refs_3_), channel_id=1, source_target_pairs={{0,8},{4,12},{8,16},{12,20},{16,24},{20,28},{24,0},{28,4},{1,9},{5... | collective-permute-start | bytes 2162696 | tf_op jit(solution)/shard_map/ppermute | solution.py:539
  221.9 35.8 %collective-permute-start.58 = (bf16[256,704]{1,0:T(8,128)(2,1)S(1)}, bf16[256,704]{1,0:T(8,128)(2,1)}, u32[]{:S(2)}, u32[]{:S(2)}) collective-permute-start(bf16[256,704]{1,0:T(8,128)(2,1)S(1)} %copy-done.12), channel_id=1, source_target_pairs={{0,8},{4,12},{8,16},{12,20},{16,24},{20,28},{24,0},{28,4},{1,9},{5... | collective-permute-start | bytes 1081352 | tf_op jit(solution)/shard_map/ppermute | solution.py:539
  229.1 32.3 %collective-permute-start.59 = (bf16[256,704]{1,0:T(8,128)(2,1)}, bf16[256,704]{1,0:T(8,128)(2,1)}, u32[]{:S(2)}, u32[]{:S(2)}) collective-permute-start(bf16[256,704]{1,0:T(8,128)(2,1)} %collective-permute-done.57.refs_3_), channel_id=1, source_target_pairs={{0,8},{4,12},{8,16},{12,20},{16,24},{20,28},{24,0},{28,4},{1,9},{5... | collective-permute-start | bytes 1081352 | tf_op jit(solution)/shard_map/ppermute | solution.py:539
  229.1 63.9 %collective-permute-start.53 = (bf16[256,1408]{1,0:T(8,128)(2,1)}, bf16[256,1408]{1,0:T(8,128)(2,1)}, u32[]{:S(2)}, u32[]{:S(2)}) collective-permute-start(bf16[256,1408]{1,0:T(8,128)(2,1)} %collective-permute-done.51.refs_4_), channel_id=1, source_target_pairs={{0,8},{4,12},{8,16},{12,20},{16,24},{20,28},{24,0},{28,4},{1,9},{5... | collective-permute-start | bytes 2162696 | tf_op jit(solution)/shard_map/ppermute | solution.py:539
  244.5 48.5 %collective-permute-start.54 = (bf16[256,1408]{1,0:T(8,128)(2,1)}, bf16[256,1408]{1,0:T(8,128)(2,1)}, u32[]{:S(2)}, u32[]{:S(2)}) collective-permute-start(bf16[256,1408]{1,0:T(8,128)(2,1)} %collective-permute-done.52.refs_5_), channel_id=1, source_target_pairs={{0,8},{4,12},{8,16},{12,20},{16,24},{20,28},{24,0},{28,4},{1,9},{5... | collective-permute-start | bytes 2162696 | tf_op jit(solution)/shard_map/ppermute | solution.py:539
  256.4 32.5 %collective-permute-start.46 = (bf16[1,2048]{1,0:T(2,128)(2,1)S(1)}, bf16[1,2048]{1,0:T(2,128)(2,1)S(1)}, u32[]{:S(2)}, u32[]{:S(2)}) collective-permute-start(bf16[1,2048]{1,0:T(2,128)(2,1)S(1)} %get-tuple-element.41), channel_id=1, source_target_pairs={{0,8},{4,12},{8,16},{12,20},{16,24},{20,28},{1,9},{5,13},{9,17},{1... | collective-permute-start | bytes 12296 | tf_op jit(solution)/shard_map/ppermute | solution.py:663
  257.7 34.5 %collective-permute-start.47 = (bf16[1,2048]{1,0:T(2,128)(2,1)S(1)}, bf16[1,2048]{1,0:T(2,128)(2,1)S(1)}, u32[]{:S(2)}, u32[]{:S(2)}) collective-permute-start(bf16[1,2048]{1,0:T(2,128)(2,1)S(1)} %get-tuple-element.42), channel_id=1, source_target_pairs={{8,0},{12,4},{16,8},{20,12},{24,16},{28,20},{9,1},{13,5},{17,9},{2... | collective-permute-start | bytes 12296 | tf_op jit(solution)/shard_map/ppermute | solution.py:664
  261.4 52.2 %collective-permute-start.60 = (bf16[256,704]{1,0:T(8,128)(2,1)}, bf16[256,704]{1,0:T(8,128)(2,1)S(1)}, u32[]{:S(2)}, u32[]{:S(2)}) collective-permute-start(bf16[256,704]{1,0:T(8,128)(2,1)} %collective-permute-done.58.refs_4_), channel_id=1, source_target_pairs={{0,8},{4,12},{8,16},{12,20},{16,24},{20,28},{24,0},{28,4},{1,9},{5... | collective-permute-start | bytes 1081352 | tf_op jit(solution)/shard_map/ppermute | solution.py:539
  288.9 24.7 %collective-permute-start.61 = (bf16[256,704]{1,0:T(8,128)(2,1)}, bf16[256,704]{1,0:T(8,128)(2,1)S(1)}, u32[]{:S(2)}, u32[]{:S(2)}) collective-permute-start(bf16[256,704]{1,0:T(8,128)(2,1)} %collective-permute-done.59.refs_5_), channel_id=1, source_target_pairs={{0,8},{4,12},{8,16},{12,20},{16,24},{20,28},{24,0},{28,4},{1,9},{5... | collective-permute-start | bytes 1081352 | tf_op jit(solution)/shard_map/ppermute | solution.py:539
  328.4 16.8 %collective-permute-start.63 = (bf16[2,320,512]{2,1,0:T(8,128)(2,1)S(1)}, bf16[2,320,512]{2,1,0:T(8,128)(2,1)S(1)}, u32[]{:S(2)}, u32[]{:S(2)}) collective-permute-start(bf16[2,320,512]{2,1,0:T(8,128)(2,1)S(1)} %slice_bitcast_fusion.1), channel_id=1, source_target_pairs={{0,4},{4,0},{8,12},{12,8},{16,20},{20,16},{24,28},{28,24},{1,5},{5... | collective-permute-start | bytes 1966088 | tf_op jit(solution)/shard_map/ppermute | solution.py:536
  329.0 16.5 %collective-permute-start.65 = (bf16[2,320,512]{2,1,0:T(8,128)(2,1)S(1)}, bf16[2,320,512]{2,1,0:T(8,128)(2,1)S(1)}, u32[]{:S(2)}, u32[]{:S(2)}) collective-permute-start(bf16[2,320,512]{2,1,0:T(8,128)(2,1)S(1)} %slice_bitcast_fusion), channel_id=1, source_target_pairs={{0,2},{1,3},{2,0},{3,1},{4,6},{5,7},{6,4},{7,5},{8,10},{9,11},{10,... | collective-permute-start | bytes 1966088 | tf_op jit(solution)/shard_map/ppermute | solution.py:542
  345.7 8.7 %collective-permute-start.64 = (bf16[320,512]{1,0:T(8,128)(2,1)S(1)}, bf16[320,512]{1,0:T(8,128)(2,1)S(1)}, u32[]{:S(2)}, u32[]{:S(2)}) collective-permute-start(bf16[320,512]{1,0:T(8,128)(2,1)S(1)} %get-tuple-element.21), channel_id=1, source_target_pairs={{0,2},{1,3},{2,0},{3,1},{4,6},{5,7},{6,4},{7,5},{8,10},{9,11},{10,... | collective-permute-start | bytes 983048 | tf_op jit(solution)/shard_map/ppermute | solution.py:542
  346.8 8.3 %collective-permute-start.66 = (bf16[320,512]{1,0:T(8,128)(2,1)S(1)}, bf16[320,512]{1,0:T(8,128)(2,1)S(1)}, u32[]{:S(2)}, u32[]{:S(2)}) collective-permute-start(bf16[320,512]{1,0:T(8,128)(2,1)S(1)} %get-tuple-element.22), channel_id=1, source_target_pairs={{0,4},{4,0},{8,12},{12,8},{16,20},{20,16},{24,28},{28,24},{1,5},{5... | collective-permute-start | bytes 983048 | tf_op jit(solution)/shard_map/ppermute | solution.py:536
  (76 other events, 935.5 us)
where the time goes:
time: 357 us; the launch traced here: 356 us
  waiting for transfers between devices  164 us (46%)
  Pallas kernels  104 us (29%)
  starting transfers between devices  51.5 us (14%)
  other arithmetic  20.9 us (6%)
  local copies, waits for them, and re-layouts  14.3 us (4%)
    ppermute x39, waiting for transfers between devices, across(): return lax.ppermute(a, 'tp', [(i, i ^ bit) for i in range(tp_size)])  68 us
    pallas_call x3, Pallas kernels, attend(): pl.pallas_call(functools.partial(attention_kernel, wide, heads, odd, pick...  56 us
    ppermute x15, waiting for transfers between devices, along(): lax.ppermute(a, 'sp', [(i, (i + 2 * k) % sp_size) for i in range(sp_size)])  50.6 us
    ppermute x1, waiting for transfers between devices, per_device(): low = lax.ppermute(rims[31:], 'sp', up_line)  26.2 us
    ppermute x39, starting transfers between devices, across(): return lax.ppermute(a, 'tp', [(i, i ^ bit) for i in range(tp_size)])  21 us
    pallas_call x1, Pallas kernels, up_and_mix(): pl.pallas_call(functools.partial(up_kernel, columns // 2, len(pieces)), o...  20.6 us
    ppermute x11, waiting for transfers between devices, mate(): return lax.ppermute(a, 'sp', [(i, i ^ 1) for i in range(sp_size)])  18.5 us
    ppermute x15, starting transfers between devices, along(): lax.ppermute(a, 'sp', [(i, (i + 2 * k) % sp_size) for i in range(sp_size)])  16.2 us
  transfers between devices with their start and end apart: 67, of which 24 were waited for; matrix products, arithmetic and copies ran while one was open for 6% of the time, Pallas kernels for 27%

commit v1 on v0

--- a/solution.py
+++ b/solution.py
@@ -227,11 +227,13 @@
     width = 2 * LANES if wide else LANES
     out = jax.ShapeDtypeStruct((tok, heads * LANES), BF16)
     kept = jax.ShapeDtypeStruct((keys, pieces[0].shape[1]), BF16)
+    row_bytes = 2 * pieces[0].shape[1] + 2 * heads * (width + LANES) + 8 * rows
+    grant = keys * row_bytes + 12 * 2**20
     return pl.pallas_call(
         functools.partial(attention_kernel, wide, heads, odd, pick, factor, rows, tile, passes),
         out_shape=(out, kept) if passes else out,
-        in_specs=[VMEM_SPEC] * 4 + [ANY_SPEC if passes else HBM_SPEC] * len(pieces),
-        out_specs=(VMEM_SPEC, HBM_SPEC) if passes else VMEM_SPEC,
+        in_specs=[VMEM_SPEC] * 4 + [ANY_SPEC] * len(pieces),
+        out_specs=(VMEM_SPEC, ANY_SPEC) if passes else VMEM_SPEC,
         scratch_shapes=[
             pltpu.VMEM((keys, pieces[0].shape[1]), BF16),
             pltpu.VMEM((tok, heads * width), BF16),
@@ -242,7 +244,7 @@
             pltpu.VMEM((rows, LANES), F32),
             pltpu.SemaphoreType.DMA((max(len(pieces), keys // tile) + 1,)),
         ],
-        compiler_params=pltpu.CompilerParams(vmem_limit_bytes=60 * 2**20),
+        compiler_params=pltpu.CompilerParams(vmem_limit_bytes=max(40 * 2**20, min(62 * 2**20, grant))),
         cost_estimate=pl.CostEstimate(flops=2 * tok * keys * heads * (width + LANES), bytes_accessed=keys * 1024, transcendentals=0),
     )(query, *tables, weights, *pieces)
 
@@ -279,7 +281,7 @@
     return pl.pallas_call(
         functools.partial(base_kernel, n, heads, first),
         out_shape=jax.ShapeDtypeStruct((total, width), BF16),
-        in_specs=[VMEM_SPEC] * heads + [HBM_SPEC] * n,
+        in_specs=[VMEM_SPEC] * heads + [ANY_SPEC] * n,
         out_specs=VMEM_SPEC,
         scratch_shapes=[
             pltpu.VMEM((n * depth, width), BF16),
@@ -287,16 +289,17 @@
         ],
         compiler_params=pltpu.CompilerParams(vmem_limit_bytes=20 * 2**20),
         cost_estimate=pl.CostEstimate(flops=2 * total * n * depth * width, bytes_accessed=10**6, transcendentals=0),
-        name="project_base",
+        name="pb",
     )(*xs, *weights)
 
 
 def norm_kernel(n, s_ref, *refs):
-    bases, (x_ref, g_ref) = refs[:2], refs[2:4]
-    weights, residuals = refs[4 : 4 + n], refs[4 + n : 4 + 2 * n]
-    a_ref, out_ref, edge_ref, o_ref, w_scr, r_scr, y_scr, sems, sems_r, sems_o = refs[4 + 2 * n :]
+    base_ref, x_ref, g_ref = refs[:3]
+    weights, residuals = refs[3 : 3 + n], refs[3 + n : 3 + 2 * n]
+    a_ref, out_ref, edge_ref, o_ref, w_scr, r_scr, y_scr, sems, sems_r, sems_o = refs[3 + 2 * n :]
     depth = weights[0].shape[0]
-    total, width = bases[0].shape
+    total, width = a_ref.shape[0], base_ref.shape[1]
+    bases = [base_ref.at[pl.ds(i * total, total)] for i in range(2)]
     copies = gather_in(weights, w_scr, [i * depth for i in range(n)], sems)
     more = gather_in(residuals, r_scr, [i * 2 * total for i in range(n)], sems_r)
     for copy in copies + more:
@@ -340,8 +343,8 @@
         put(i).wait()
 
 
-def project_norm(places, bases, x, gain, weights, residuals):
-    total, width = bases[0].shape
+def project_norm(places, base, x, gain, weights, residuals):
+    total, width = base.shape[0] // 2, base.shape[1]
     n = len(weights)
     own = residuals[0].shape[1]
     rows = 128 if total % 128 == 0 else total
@@ -352,7 +355,7 @@
             jax.ShapeDtypeStruct((2 * total, width), BF16),
             jax.ShapeDtypeStruct((32, width), BF16),
         ),
-        in_specs=[SMEM_SPEC] + [VMEM_SPEC] * 4 + [HBM_SPEC] * (2 * n),
+        in_specs=[SMEM_SPEC] + [VMEM_SPEC] * 3 + [ANY_SPEC] * (2 * n),
         out_specs=(VMEM_SPEC, HBM_SPEC, VMEM_SPEC),
         scratch_shapes=[
             pltpu.VMEM((2 * total, width), BF16),
@@ -365,49 +368,45 @@
         ],
         compiler_params=pltpu.CompilerParams(vmem_limit_bytes=28 * 2**20),
         cost_estimate=pl.CostEstimate(flops=4 * total * n * weights[0].shape[0] * width, bytes_accessed=10**6, transcendentals=0),
-        name="project_norm",
-    )(places, *bases, x, gain, *weights, *residuals)
+        name="pn",
+    )(places, base, x, gain, *weights, *residuals)
 
 
 def up_kernel(half, n, s_ref, in_ref, edge_ref, t_ref, *refs):
     pieces = refs[:n]
-    o_ref, x_ref, w_scr, u_scr, e_scr, sems, sems_x = refs[n:]
+    o_ref, x_scr, w_scr, u_scr, sems, sems_x = refs[n:]
     block = pieces[0].shape[0]
     copies = gather_in(pieces, w_scr, [pl.multiple_of(s_ref[i], block) for i in range(n)], sems)
-    total = x_ref.shape[0]
+    total = in_ref.shape[0]
     rows = 256 if total % 256 == 0 else total
+    rim = edge_ref.shape[0]
 
     def take(i):
-        at = pl.ds(pl.multiple_of(i * rows, rows), rows)
-        return pltpu.make_async_copy(in_ref.at[at], x_ref.at[at], sems_x.at[i])
+        at = pl.multiple_of(i * rows, rows)
+        to = pl.multiple_of(at + rim, rim)
+        return pltpu.make_async_copy(in_ref.at[pl.ds(at, rows)], x_scr.at[pl.ds(to, rows)], sems_x.at[i])
 
     for i in range(total // rows):
         take(i).start()
+    x_scr[:rim, :] = edge_ref[...]
     for copy in copies:
         copy.wait()
     part = 64
     per, last = rows // part, total // part - 1
-    e_scr[...] = (
-        jnp.dot(edge_ref[...], w_scr[...], preferred_element_type=F32).astype(BF16).astype(F32)
-    )
     row = lax.broadcasted_iota(jnp.int32, (part, 2 * half), 0)
 
     def multiply(i):
         take(i).wait()
-        r = pl.multiple_of(i * rows, rows)
-        u_scr[pl.ds(r, rows), :] = jnp.dot(
-            x_ref[pl.ds(r, rows), :], w_scr[...], preferred_element_type=F32
-        ).astype(BF16)
+        first = isinstance(i, int) and i == 0
+        at = pl.ds(0, rows + rim) if first else pl.ds(pl.multiple_of(i * rows + rim, rim), rows)
+        u_scr[at, :] = jnp.dot(x_scr[at, :], w_scr[...], preferred_element_type=F32).astype(BF16)
 
     def mix(i):
         r = pl.multiple_of(i * part, part)
-        cur = u_scr[pl.ds(r, part), :].astype(F32)
-        up_at = pl.multiple_of(jnp.maximum(r - 16, 0), 16)
-        down_at = pl.multiple_of(jnp.minimum(r + part, total - 16), 16)
-        above = u_scr[pl.ds(up_at, 16), :].astype(F32)[15:16]
-        below = u_scr[pl.ds(down_at, 16), :].astype(F32)[0:1]
-        above = jnp.where(i == 0, e_scr[0:1, :], above)
-        below = jnp.where(i == last, e_scr[1:2, :], below)
+        cur = u_scr[pl.ds(pl.multiple_of(r + rim, rim), part), :].astype(F32)
+        down_at = pl.multiple_of(jnp.where(i == last, 0, r + part + rim), rim)
+        above = u_scr[pl.ds(pl.multiple_of(r, rim), rim), :].astype(F32)[rim - 1 :]
+        below = u_scr[pl.ds(down_at, rim), :].astype(F32)[:1]
         before = jnp.where(row == 0, above, pltpu.roll(cur, 1, 0))
         after = jnp.where(row == part - 1, below, pltpu.roll(cur, part - 1, 0))
         smooth = t_ref[0:1, :] * before + t_ref[1:2, :] * cur + t_ref[2:3, :] * after
@@ -444,27 +443,26 @@
         in_specs=[SMEM_SPEC, HBM_SPEC] + [VMEM_SPEC] * 2 + [HBM_SPEC] * len(pieces),
         out_specs=VMEM_SPEC,
         scratch_shapes=[
-            pltpu.VMEM((total, width), BF16),
+            pltpu.VMEM((total + 16, width), BF16),
             pltpu.VMEM((width, columns), BF16),
-            pltpu.VMEM((total, columns), BF16),
-            pltpu.VMEM((16, columns), F32),
+            pltpu.VMEM((total + 16, columns), BF16),
             pltpu.SemaphoreType.DMA((len(pieces),)),
             pltpu.SemaphoreType.DMA((total // (256 if total % 256 == 0 else total),)),
         ],
         compiler_params=pltpu.CompilerParams(vmem_limit_bytes=60 * 2**20),
         cost_estimate=pl.CostEstimate(flops=2 * total * width * columns, bytes_accessed=10**6, transcendentals=0),
-        name="up_and_mix",
+        name="mx",
     )(places, normed, edge, taps, *pieces)
 
 
-def down_kernel(n, s_ref, h_ref, *refs):
+def down_kernel(n, base, s_ref, h_ref, *refs):
     pieces = refs[:n]
-    keep_ref, send_ref, d_scr, sems = refs[n:]
+    o_ref, d_scr, sems = refs[n:]
     block = pieces[0].shape[0]
     copies = gather_in(pieces, d_scr, [pl.multiple_of(s_ref[i], block) for i in range(n)], sems)
     for copy in copies:
         copy.wait()
-    far, _, tok, width = keep_ref.shape
+    far, _, tok, width = o_ref.shape
     side = s_ref[n]
     rows = tok // 2 if tok % 32 == 0 else tok
     steps = tok // rows
@@ -474,34 +472,30 @@
         r = pl.multiple_of((i - rel * steps) * rows, rows)
         own = jnp.where(rel == 0, side, 1 - side)
         h = h_ref[pl.ds(pl.multiple_of(own * tok + r, rows), rows), :]
-        for o in range(2 * far):
-            out = lax.dot_general(
-                h,
-                d_scr[o * width : (o + 1) * width, :],
-                (((1,), (1,)), ((), ())),
-                preferred_element_type=F32,
+        for o in range(far):
+            at = (base + o) * width
+            o_ref[o, rel, pl.ds(r, rows), :] = lax.dot_general(
+                h, d_scr[at : at + width, :], (((1,), (1,)), ((), ())), preferred_element_type=F32
             ).astype(BF16)
-            ref = keep_ref if o < far else send_ref
-            ref[o % far, rel, pl.ds(r, rows), :] = out
         return c
 
     lax.fori_loop(0, 2 * steps, multiply, 0)
 
 
-def down_terms(places, hidden, pieces, tp_size, tok, width):
-    shape = jax.ShapeDtypeStruct((tp_size // 2, 2, tok, width), BF16)
+def down_terms(places, hidden, pieces, tp_size, tok, width, base):
+    far = tp_size // 2
     return pl.pallas_call(
-        functools.partial(down_kernel, len(pieces)),
-        out_shape=(shape, shape),
+        functools.partial(down_kernel, len(pieces), base),
+        out_shape=jax.ShapeDtypeStruct((far, 2, tok, width), BF16),
         in_specs=[SMEM_SPEC, VMEM_SPEC] + [HBM_SPEC] * len(pieces),
-        out_specs=(VMEM_SPEC, VMEM_SPEC),
+        out_specs=VMEM_SPEC,
         scratch_shapes=[
             pltpu.VMEM((tp_size * width, hidden.shape[1]), BF16),
             pltpu.SemaphoreType.DMA((len(pieces),)),
         ],
         compiler_params=pltpu.CompilerParams(vmem_limit_bytes=18 * 2**20),
-        cost_estimate=pl.CostEstimate(flops=2 * hidden.size * tp_size * width, bytes_accessed=10**6, transcendentals=0),
-        name="down_terms",
+        cost_estimate=pl.CostEstimate(flops=hidden.size * tp_size * width, bytes_accessed=10**6, transcendentals=0),
+        name="dt",
     )(places, hidden, *pieces)
 
 
@@ -654,15 +648,13 @@
     full_w = over_tp(paired(heads_w, mate(heads_w)), 1)
     full_n = over_tp(paired(heads_n, mate(heads_n)), 1)
     lanes_at = jnp.stack(lanes_at + [tp * own_width, side]).astype(jnp.int32)
-    bases = []
-    for i in range(2):
-        bases.append(project_base([full_w], outs_w, i * tok_rows, tok_rows))
-    attended, normed, rims = project_norm(lanes_at, bases, full_n, full_gain, outs_n, residuals)
+    base = project_base([full_w], outs_w, 0, 2 * tok_rows)
+    attended, normed, rims = project_norm(lanes_at, base, full_n, full_gain, outs_n, residuals)
 
     up_line = [(i, i + 2) for i in range(sp_size - 2)]
     low = lax.ppermute(rims[31:], "sp", up_line)
     high = lax.ppermute(rims[:1], "sp", [(b, a) for a, b in up_line])
-    edge = jnp.concatenate([low, high, jnp.zeros((14, normed.shape[1]), BF16)], axis=0)
+    edge = jnp.concatenate([high, jnp.zeros((14, normed.shape[1]), BF16), low], axis=0)
     block = up_gate.shape[0]
     position = me // 2
     starts, blocks = [], []
@@ -679,9 +671,9 @@
     taps = jnp.where(side == 0, conv_taps[:, :, :half], conv_taps[:, :, half:]).reshape(3, 2 * half)
     taps = jnp.pad(taps, ((0, 5), (0, 0)))
     hidden = up_and_mix(jnp.stack(starts).astype(jnp.int32), normed, edge, taps, up_pieces)
-    kept, sent = down_terms(
-        jnp.stack(blocks + [side]).astype(jnp.int32), hidden, down_pieces, tp_size, tok_rows, own_width
-    )
+    at = jnp.stack(blocks + [side]).astype(jnp.int32)
+    sent = down_terms(at, hidden, down_pieces, tp_size, tok_rows, own_width, tp_size // 2)
+    kept = down_terms(at, hidden, down_pieces, tp_size, tok_rows, own_width, 0)
 
     def add(a, b):
         return (a.astype(F32) + b.astype(F32)).astype(BF16)

time: 357 us -> 366 us (1.025)
  starting transfers between devices: 51.5 us -> 68.6 us
  other arithmetic: 20.9 us -> 14.6 us
    ppermute x1, waiting for transfers between devices: 26.2 us -> 0.01 us  [per_device(): low = lax.ppermute(rims[31:], 'sp', up_line)]
    ppermute x1, waiting for transfers between devices: 0.89 us -> 26.2 us  [per_device(): high = lax.ppermute(rims[:1], 'sp', [(b, a) for a, b in up_line])]
    ppermute x11, starting transfers between devices: 11.8 us -> 23.9 us  [mate(): return lax.ppermute(a, 'sp', [(i, i ^ 1) for i in range(sp_size)])]
    pallas_call x1 -> x2, Pallas kernels: 7.27 us -> 10.8 us  [down_terms(): pl.pallas_call(functools.partial(down_kernel, len(pieces), base), out_sha...]
    pallas_call x2 -> x1, Pallas kernels: 10.6 us -> 8.42 us  [project_base(): pl.pallas_call(functools.partial(base_kernel, n, heads, first), out_shape...]
    unnamed x115 -> x79, local copies, waits for them, and re-layouts: 7.2 us -> 8.86 us
  transfers between devices with their start and end apart: 67 -> 67, of which waited for: 24 -> 20; matrix products, arithmetic and copies ran while one was open for 6% -> 3% of each run, Pallas kernels for 27% -> 27%
where the time goes in v1:
time: 366 us; the launch traced here: 365 us
  waiting for transfers between devices  162 us (44%)
  Pallas kernels  104 us (28%)
  starting transfers between devices  68.6 us (19%)
  other arithmetic  14.6 us (4%)
  local copies, waits for them, and re-layouts  14.5 us (4%)
    ppermute x39, waiting for transfers between devices, across(): return lax.ppermute(a, 'tp', [(i, i ^ bit) for i in range(tp_size)])  65.4 us
    pallas_call x3, Pallas kernels, attend(): pl.pallas_call(functools.partial(attention_kernel, wide, heads, odd, pick...  54.5 us
    ppermute x15, waiting for transfers between devices, along(): lax.ppermute(a, 'sp', [(i, (i + 2 * k) % sp_size) for i in range(sp_size)])  50.6 us
    ppermute x1, waiting for transfers between devices, per_device(): high = lax.ppermute(rims[:1], 'sp', [(b, a) for a, b in up_line])  26.2 us
    ppermute x11, starting transfers between devices, mate(): return lax.ppermute(a, 'sp', [(i, i ^ 1) for i in range(sp_size)])  23.9 us
    ppermute x39, starting transfers between devices, across(): return lax.ppermute(a, 'tp', [(i, i ^ bit) for i in range(tp_size)])  22.3 us
    ppermute x11, waiting for transfers between devices, mate(): return lax.ppermute(a, 'sp', [(i, i ^ 1) for i in range(sp_size)])  19.9 us
    pallas_call x1, Pallas kernels, up_and_mix(): pl.pallas_call(functools.partial(up_kernel, columns // 2, len(pieces)), o...  19.6 us
  transfers between devices with their start and end apart: 67, of which 20 were waited for; matrix products, arithmetic and copies ran while one was open for 3% of the time, Pallas kernels for 27%

profile of v1, /device:TPU:0, one launch (start us, length us, event | category | flops | bytes accessed | tf_op | source)
XLA Modules:
  0.0 365.1 jit_solution(15967796928029034535)
XLA Ops:
  2.7 2.3 fusion.15
  5.0 1.9 concatenate.71.refs_4_
  7.0 3.1 collective-permute-start
  10.1 1.5 collective-permute-start.12
  11.6 5.6 %collective-permute-done.refs_5_ = bf16[160,640]{1,0:T(8,128)(2,1)S(1)} collective-permute-done((bf16[160,640]{1,0:T(8,128)(2,1)S(1)}, bf16[160,640]{1,0:T(8,128)(2,1)S(1)}, u32[]{:S(2)}, u32[]{:S(2)}) %collective-permute-start) | collective-permute-done | bytes 204832 | tf_op jit(solution)/shard_map/ppermute | solution.py:533
  17.2 1.5 collective-permute-start.37
  18.7 1.5 collective-permute-start.16
  20.8 1.6 collective-permute-start.13
  22.4 2.9 collective-permute-done.4.refs_9_
  25.2 1.9 fusion.16
  28.6 1.5 collective-permute-start.5
  31.6 4.8 %collective-permute-done.8.refs_13_ = bf16[160,640]{1,0:T(8,128)(2,1)S(1)} collective-permute-done((bf16[160,640]{1,0:T(8,128)(2,1)S(1)}, bf16[160,640]{1,0:T(8,128)(2,1)S(1)}, u32[]{:S(2)}, u32[]{:S(2)}) %collective-permute-start.8) | collective-permute-done | bytes 204832 | tf_op jit(solution)/shard_map/ppermute | solution.py:533
  38.3 1.8 collective-permute-done.17.refs_22_
  40.1 1.5 collective-permute-start.9
  44.4 2.8 collective-permute-done.9.refs_14_
  47.2 2.4 collective-permute-start.25
  49.7 1.8 collective-permute-done.21.refs_26_
  52.6 2.6 collective-permute-done.25.refs_30_
  55.5 1.7 collective-permute-start.39
  57.3 1.5 collective-permute-start.55
  59.0 30.4 %shard_map.145 = (bf16[640,256]{1,0:T(8,128)(2,1)S(1)}, bf16[5120,640]{1,0:T(8,128)(2,1)}) custom-call(bf16[640,384]{1,0:T(8,128)(2,1)S(1)} %copy-done.12, f32[640,128]{1,0:T(8,128)S(1)} %get-tuple-element.33.refs_1_, f32[640,128]{1,0:T(8,128)S(1)} %get-tuple-element.22.refs_2_, bf16[512,512]{1,0:T(8,128)(2,1)S(1)} %copy-done.11, ...), custom_call_target="tpu_custom_call" | custom-call | flops 5033164800 | bytes 5242880 | tf_op jit(solution)/shard_map/pallas_call | solution.py:232
  90.2 1.5 collective-permute-start.48
  91.8 2.9 copy-done
  94.6 12.1 %shard_map.146 = bf16[640,128]{1,0:T(8,128)(2,1)S(1)} custom-call(bf16[640,128]{1,0:T(8,128)(2,1)S(1)} %get-tuple-element.32.refs_0_, f32[640,128]{1,0:T(8,128)S(1)} %get-tuple-element.34.refs_1_, f32[640,128]{1,0:T(8,128)S(1)} %get-tuple-element.21.refs_2_, bf16[512,128]{1,0:T(8,128)(2,1)S(1)} %get-tuple-element.36.refs_3_, bf16[5120,640]{1,0:T(8,128)(2,1)S(1)} %copy-done), custom_call_target="tpu_custom_call" | custom-call | flops 1677721600 | bytes 5242880 | tf_op jit(solution)/shard_map/pallas_call | solution.py:232
  107.8 1.6 collective-permute-start.29
  109.3 12.0 %shard_map.147 = bf16[640,128]{1,0:T(8,128)(2,1)S(1)} custom-call(bf16[640,128]{1,0:T(8,128)(2,1)S(1)} %get-tuple-element.31.refs_0_, f32[640,128]{1,0:T(8,128)S(1)} %get-tuple-element.34.refs_1_, f32[640,128]{1,0:T(8,128)S(1)} %get-tuple-element.21.refs_2_, bf16[512,128]{1,0:T(8,128)(2,1)S(1)} %get-tuple-element.35.refs_3_, bf16[5120,640]{1,0:T(8,128)(2,1)S(1)} %copy-done), custom_call_target="tpu_custom_call" | custom-call | flops 1677721600 | bytes 5242880 | tf_op jit(solution)/shard_map/pallas_call | solution.py:232
  123.8 3.6 collective-permute-done.34
  127.3 1.5 collective-permute-start.43
  129.6 3.7 %collective-permute-start.57 = (bf16[256,704]{1,0:T(8,128)(2,1)S(1)}, bf16[256,704]{1,0:T(8,128)(2,1)S(1)}, u32[]{:S(2)}, u32[]{:S(2)}) collective-permute-start(bf16[256,704]{1,0:T(8,128)(2,1)S(1)} %collective-permute-done.55.refs_1_), channel_id=1, source_target_pairs={{0,8},{4,12},{8,16},{12,20},{16,24},{20,28},{24,0},{28,4},{1,9},{5... | collective-permute-start | bytes 1081352 | tf_op jit(solution)/shard_map/ppermute | solution.py:533
  134.5 47.3 %collective-permute-done.35 = bf16[1280,128]{1,0:T(8,128)(2,1)S(1)} collective-permute-done((bf16[1280,128]{1,0:T(8,128)(2,1)S(1)}, bf16[1280,128]{1,0:T(8,128)(2,1)S(1)}, u32[]{:S(2)}, u32[]{:S(2)}) %collective-permute-start.35) | collective-permute-done | bytes 327712 | tf_op jit(solution)/shard_map/ppermute | solution.py:536
  184.8 3.8 %collective-permute-start.50 = (bf16[256,1408]{1,0:T(8,128)(2,1)}, bf16[256,1408]{1,0:T(8,128)(2,1)S(1)}, u32[]{:S(2)}, u32[]{:S(2)}) collective-permute-start(bf16[256,1408]{1,0:T(8,128)(2,1)} %copy-done.35), channel_id=1, source_target_pairs={{0,8},{4,12},{8,16},{12,20},{16,24},{20,28},{24,0},{28,4},{1,9},{5... | collective-permute-start | bytes 2162696 | tf_op jit(solution)/shard_map/ppermute | solution.py:533
  190.5 14.8 %collective-permute-done.50.refs_3_ = bf16[256,1408]{1,0:T(8,128)(2,1)S(1)} collective-permute-done((bf16[256,1408]{1,0:T(8,128)(2,1)}, bf16[256,1408]{1,0:T(8,128)(2,1)S(1)}, u32[]{:S(2)}, u32[]{:S(2)}) %collective-permute-start.50) | collective-permute-done | bytes 720928 | tf_op jit(solution)/shard_map/ppermute | solution.py:533
  205.4 2.0 collective-permute-start.51
  208.0 1.6 pad_maximum_fusion.refs_0_
  209.7 8.4 %pb.1.refs_0_ = bf16[1280,2048]{1,0:T(8,128)(2,1)S(1)} custom-call(bf16[1280,1024]{1,0:T(8,128)(2,1)S(1)} %pad_maximum_fusion.refs_0_, bf16[256,2048]{1,0:T(8,128)(2,1)} %refs_1_.1, bf16[256,2048]{1,0:T(8,128)(2,1)} %collective-permute-done.31.refs_2_, bf16[256,2048]{1,0:T(8,128)(2,1)} %collective-permute-done.32.refs_3_, ...), custom_call_target="tpu_custom_call" | custom-call | flops 5368709120 | bytes 1000000 | tf_op jit(solution)/shard_map/pb/pallas_call | solution.py:281
  218.5 7.8 %collective-permute-done.51.refs_4_ = bf16[256,1408]{1,0:T(8,128)(2,1)} collective-permute-done((bf16[256,1408]{1,0:T(8,128)(2,1)S(1)}, bf16[256,1408]{1,0:T(8,128)(2,1)}, u32[]{:S(2)}, u32[]{:S(2)}) %collective-permute-start.51) | collective-permute-done | bytes 720928 | tf_op jit(solution)/shard_map/ppermute | solution.py:533
  227.1 14.7 %collective-permute-done.52.refs_5_ = bf16[256,1408]{1,0:T(8,128)(2,1)} collective-permute-done((bf16[256,1408]{1,0:T(8,128)(2,1)S(1)}, bf16[256,1408]{1,0:T(8,128)(2,1)}, u32[]{:S(2)}, u32[]{:S(2)}) %collective-permute-start.52) | collective-permute-done | bytes 720928 | tf_op jit(solution)/shard_map/ppermute | solution.py:533
  241.9 10.6 %pn.1 = (bf16[640,512]{1,0:T(8,128)(2,1)S(1)}, bf16[1280,2048]{1,0:T(8,128)(2,1)S(1)}, bf16[32,2048]{1,0:T(8,128)(2,1)S(1)}) custom-call(s32[6]{0:T(128)S(1)} %stack.79.s_ref, bf16[1280,2048]{1,0:T(8,128)(2,1)S(1)} %pb.1.refs_0_, bf16[1280,512]{1,0:T(8,128)(2,1)S(1)} %pad_maximum_fusion.2.refs_1_, f32[1,2048]{1,0:T(1,128)S(1)} %slice_dynamic-update-slice_fusion.refs_2_, ...), custom_call_target="tpu_custom_call" | custom-call | flops 2684354560 | bytes 1000000 | tf_op jit(solution)/shard_map/pn/pallas_call | solution.py:351
  253.3 2.4 copy-done.10
  257.0 4.5 %collective-permute-start.47 = (bf16[1,2048]{1,0:T(2,128)(2,1)S(1)}, bf16[1,2048]{1,0:T(2,128)(2,1)S(1)}, u32[]{:S(2)}, u32[]{:S(2)}) collective-permute-start(bf16[1,2048]{1,0:T(2,128)(2,1)S(1)} %get-tuple-element.38), channel_id=1, source_target_pairs={{0,8},{4,12},{8,16},{12,20},{16,24},{20,28},{1,9},{5,13},{9,17},{1... | collective-permute-start | bytes 12296 | tf_op jit(solution)/shard_map/ppermute | solution.py:655
  263.3 26.2 %collective-permute-done.46 = bf16[1,2048]{1,0:T(2,128)(2,1)S(1)} collective-permute-done((bf16[1,2048]{1,0:T(2,128)(2,1)S(1)}, bf16[1,2048]{1,0:T(2,128)(2,1)S(1)}, u32[]{:S(2)}, u32[]{:S(2)}) %collective-permute-start.46) | collective-permute-done | bytes 4128 | tf_op jit(solution)/shard_map/ppermute | solution.py:656
  290.8 19.6 %mx.1.h_ref = bf16[1280,704]{1,0:T(8,128)(2,1)} custom-call(s32[8]{0:T(128)} %stack.97.s_ref, bf16[1280,2048]{1,0:T(8,128)(2,1)} %copy-done.10, bf16[16,2048]{1,0:T(8,128)(2,1)} %pad_maximum_fusion.11.edge_ref, f32[8,1408]{1,0:T(8,128)} %pad.4.t_ref, bf16[256,1408]{1,0:T(8,128)(2,1)} %copy-done.28, bf16[256,1408]{1,0:T(8,128)(2,1)} %copy-done.35, ...), custom_call_target="tpu_custom_call" | custom-call | flops 7381975040 | bytes 1000000 | tf_op jit(solution)/shard_map/mx/pallas_call | solution.py:440
  310.4 1.5 copy-done.1
  312.0 5.4 %dt.3 = bf16[2,2,640,512]{3,2,1,0:T(8,128)(2,1)S(1)} custom-call(s32[9]{0:T(128)S(1)} %stack.88.s_ref, bf16[1280,704]{1,0:T(8,128)(2,1)S(1)} %copy-done.1, bf16[256,704]{1,0:T(8,128)(2,1)S(1)} %get-tuple-element.24.refs_0_, bf16[256,704]{1,0:T(8,128)(2,1)S(1)} %collective-permute-done.55.refs_1_, bf16[256,704]{1,0:T(8,128)(2,1)S(1)} %collective-permute-done.56.refs_2_, ...), custom_call_target="tpu_custom_call" | custom-call | flops 1845493760 | bytes 1000000 | tf_op jit(solution)/shard_map/dt/pallas_call | solution.py:487
  317.4 5.4 %dt.2 = bf16[2,2,640,512]{3,2,1,0:T(8,128)(2,1)S(1)} custom-call(s32[9]{0:T(128)S(1)} %stack.88.s_ref, bf16[1280,704]{1,0:T(8,128)(2,1)S(1)} %copy-done.1, bf16[256,704]{1,0:T(8,128)(2,1)S(1)} %get-tuple-element.24.refs_0_, bf16[256,704]{1,0:T(8,128)(2,1)S(1)} %collective-permute-done.55.refs_1_, bf16[256,704]{1,0:T(8,128)(2,1)S(1)} %collective-permute-done.56.refs_2_, ...), custom_call_target="tpu_custom_call" | custom-call | flops 1845493760 | bytes 1000000 | tf_op jit(solution)/shard_map/dt/pallas_call | solution.py:487
  323.8 12.9 %collective-permute-start.63 = (bf16[2,320,512]{2,1,0:T(8,128)(2,1)S(1)}, bf16[2,320,512]{2,1,0:T(8,128)(2,1)S(1)}, u32[]{:S(2)}, u32[]{:S(2)}) collective-permute-start(bf16[2,320,512]{2,1,0:T(8,128)(2,1)S(1)} %slice_bitcast_fusion.1), channel_id=1, source_target_pairs={{0,4},{4,0},{8,12},{12,8},{16,20},{20,16},{24,28},{28,24},{1,5},{5... | collective-permute-start | bytes 1966088 | tf_op jit(solution)/shard_map/ppermute | solution.py:530
  338.0 14.1 %collective-permute-done.63 = bf16[2,320,512]{2,1,0:T(8,128)(2,1)S(1)} collective-permute-done((bf16[2,320,512]{2,1,0:T(8,128)(2,1)S(1)}, bf16[2,320,512]{2,1,0:T(8,128)(2,1)S(1)}, u32[]{:S(2)}, u32[]{:S(2)}) %collective-permute-start.63) | collective-permute-done | bytes 655392 | tf_op jit(solution)/shard_map/ppermute | solution.py:530
  356.4 6.4 %collective-permute-done.64 = bf16[320,512]{1,0:T(8,128)(2,1)S(1)} collective-permute-done((bf16[320,512]{1,0:T(8,128)(2,1)S(1)}, bf16[320,512]{1,0:T(8,128)(2,1)S(1)}, u32[]{:S(2)}, u32[]{:S(2)}) %collective-permute-start.64) | collective-permute-done | bytes 327712 | tf_op jit(solution)/shard_map/ppermute | solution.py:536
  (222 shorter events, 38.9 us)
Async XLA Ops:
  7.0 10.2 %collective-permute-start = (bf16[160,640]{1,0:T(8,128)(2,1)S(1)}, bf16[160,640]{1,0:T(8,128)(2,1)S(1)}, u32[]{:S(2)}, u32[]{:S(2)}) collective-permute-start(bf16[160,640]{1,0:T(8,128)(2,1)S(1)} %constant_dynamic-slice_fusion), channel_id=1, source_target_pairs={{0,8},{4,12},{8,16},{12,20},{16,24},{20,28},{24,0},{28,4},{1,9},{5... | collective-permute-start | bytes 614408 | tf_op jit(solution)/shard_map/ppermute | solution.py:533
  10.1 10.7 %collective-permute-start.12 = (bf16[160,640]{1,0:T(8,128)(2,1)S(1)}, bf16[160,640]{1,0:T(8,128)(2,1)S(1)}, u32[]{:S(2)}, u32[]{:S(2)}) collective-permute-start(bf16[160,640]{1,0:T(8,128)(2,1)S(1)} %constant_dynamic-slice_fusion), channel_id=1, source_target_pairs={{0,4},{4,0},{8,12},{12,8},{16,20},{20,16},{24,28},{28,24},{1,5},{5... | collective-permute-start | bytes 614408 | tf_op jit(solution)/shard_map/ppermute | solution.py:530
  17.2 8.0 %collective-permute-start.4 = (bf16[160,640]{1,0:T(8,128)(2,1)S(1)}, bf16[160,640]{1,0:T(8,128)(2,1)S(1)}, u32[]{:S(2)}, u32[]{:S(2)}) collective-permute-start(bf16[160,640]{1,0:T(8,128)(2,1)S(1)} %collective-permute-done.refs_5_), channel_id=1, source_target_pairs={{0,8},{4,12},{8,16},{12,20},{16,24},{20,28},{24,0},{28,4},{1,9},{5... | collective-permute-start | bytes 614408 | tf_op jit(solution)/shard_map/ppermute | solution.py:533
  18.7 8.4 %collective-permute-start.16 = (bf16[160,640]{1,0:T(8,128)(2,1)S(1)}, bf16[160,640]{1,0:T(8,128)(2,1)S(1)}, u32[]{:S(2)}, u32[]{:S(2)}) collective-permute-start(bf16[160,640]{1,0:T(8,128)(2,1)S(1)} %collective-permute-done.refs_5_), channel_id=1, source_target_pairs={{0,4},{4,0},{8,12},{12,8},{16,20},{20,16},{24,28},{28,24},{1,5},{5... | collective-permute-start | bytes 614408 | tf_op jit(solution)/shard_map/ppermute | solution.py:530
  20.8 9.6 %collective-permute-start.13 = (bf16[160,640]{1,0:T(8,128)(2,1)S(1)}, bf16[160,640]{1,0:T(8,128)(2,1)S(1)}, u32[]{:S(2)}, u32[]{:S(2)}) collective-permute-start(bf16[160,640]{1,0:T(8,128)(2,1)S(1)} %collective-permute-done.12.refs_17_), channel_id=1, source_target_pairs={{0,2},{1,3},{2,0},{3,1},{4,6},{5,7},{6,4},{7,5},{8,10},{9,11},{10,... | collective-permute-start | bytes 614408 | tf_op jit(solution)/shard_map/ppermute | solution.py:536
  27.1 9.3 %collective-permute-start.8 = (bf16[160,640]{1,0:T(8,128)(2,1)S(1)}, bf16[160,640]{1,0:T(8,128)(2,1)S(1)}, u32[]{:S(2)}, u32[]{:S(2)}) collective-permute-start(bf16[160,640]{1,0:T(8,128)(2,1)S(1)} %collective-permute-done.4.refs_9_), channel_id=1, source_target_pairs={{0,8},{4,12},{8,16},{12,20},{16,24},{20,28},{24,0},{28,4},{1,9},{5... | collective-permute-start | bytes 614408 | tf_op jit(solution)/shard_map/ppermute | solution.py:533
  28.1 8.3 %collective-permute-start.20 = (bf16[160,640]{1,0:T(8,128)(2,1)S(1)}, bf16[160,640]{1,0:T(8,128)(2,1)S(1)}, u32[]{:S(2)}, u32[]{:S(2)}) collective-permute-start(bf16[160,640]{1,0:T(8,128)(2,1)S(1)} %collective-permute-done.4.refs_9_), channel_id=1, source_target_pairs={{0,4},{4,0},{8,12},{12,8},{16,20},{20,16},{24,28},{28,24},{1,5},{5... | collective-permute-start | bytes 614408 | tf_op jit(solution)/shard_map/ppermute | solution.py:530
  28.6 8.3 %collective-permute-start.5 = (bf16[160,640]{1,0:T(8,128)(2,1)S(1)}, bf16[160,640]{1,0:T(8,128)(2,1)S(1)}, u32[]{:S(2)}, u32[]{:S(2)}) collective-permute-start(bf16[160,640]{1,0:T(8,128)(2,1)S(1)} %collective-permute-done.4.refs_9_), channel_id=1, source_target_pairs={{0,2},{1,3},{2,0},{3,1},{4,6},{5,7},{6,4},{7,5},{8,10},{9,11},{10,... | collective-permute-start | bytes 614408 | tf_op jit(solution)/shard_map/ppermute | solution.py:536
  30.4 9.7 %collective-permute-start.17 = (bf16[160,640]{1,0:T(8,128)(2,1)S(1)}, bf16[160,640]{1,0:T(8,128)(2,1)S(1)}, u32[]{:S(2)}, u32[]{:S(2)}) collective-permute-start(bf16[160,640]{1,0:T(8,128)(2,1)S(1)} %collective-permute-done.16.refs_21_), channel_id=1, source_target_pairs={{0,2},{1,3},{2,0},{3,1},{4,6},{5,7},{6,4},{7,5},{8,10},{9,11},{10,... | collective-permute-start | bytes 614408 | tf_op jit(solution)/shard_map/ppermute | solution.py:536
  42.4 9.2 %collective-permute-start.10 = (bf16[160,640]{1,0:T(8,128)(2,1)S(1)}, bf16[160,640]{1,0:T(8,128)(2,1)S(1)}, u32[]{:S(2)}, u32[]{:S(2)}) collective-permute-start(bf16[160,640]{1,0:T(8,128)(2,1)S(1)} %collective-permute-done.8.refs_13_), channel_id=1, source_target_pairs={{0,1},{1,0},{2,3},{3,2},{4,5},{5,4},{6,7},{7,6},{8,9},{9,8},{10,11... | collective-permute-start | bytes 614408 | tf_op jit(solution)/shard_map/ppermute | solution.py:536
  42.5 9.1 %collective-permute-start.21 = (bf16[160,640]{1,0:T(8,128)(2,1)S(1)}, bf16[160,640]{1,0:T(8,128)(2,1)S(1)}, u32[]{:S(2)}, u32[]{:S(2)}) collective-permute-start(bf16[160,640]{1,0:T(8,128)(2,1)S(1)} %collective-permute-done.20.refs_25_), channel_id=1, source_target_pairs={{0,2},{1,3},{2,0},{3,1},{4,6},{5,7},{6,4},{7,5},{8,10},{9,11},{10,... | collective-permute-start | bytes 614408 | tf_op jit(solution)/shard_map/ppermute | solution.py:536
  43.1 9.0 %collective-permute-start.22 = (bf16[160,640]{1,0:T(8,128)(2,1)S(1)}, bf16[160,640]{1,0:T(8,128)(2,1)S(1)}, u32[]{:S(2)}, u32[]{:S(2)}) collective-permute-start(bf16[160,640]{1,0:T(8,128)(2,1)S(1)} %collective-permute-done.20.refs_25_), channel_id=1, source_target_pairs={{0,1},{1,0},{2,3},{3,2},{4,5},{5,4},{6,7},{7,6},{8,9},{9,8},{10,11... | collective-permute-start | bytes 614408 | tf_op jit(solution)/shard_map/ppermute | solution.py:536
  47.2 8.0 %collective-permute-start.25 = (bf16[160,640]{1,0:T(8,128)(2,1)S(1)}, bf16[160,640]{1,0:T(8,128)(2,1)S(1)}, u32[]{:S(2)}, u32[]{:S(2)}) collective-permute-start(bf16[160,640]{1,0:T(8,128)(2,1)S(1)} %collective-permute-done.24.refs_29_), channel_id=1, source_target_pairs={{0,2},{1,3},{2,0},{3,1},{4,6},{5,7},{6,4},{7,5},{8,10},{9,11},{10,... | collective-permute-start | bytes 614408 | tf_op jit(solution)/shard_map/ppermute | solution.py:536
  55.2 66.8 %collective-permute-start.42 = (bf16[640,512]{1,0:T(8,128)(2,1)S(1)}, bf16[640,512]{1,0:T(8,128)(2,1)S(1)}, u32[]{:S(2)}, u32[]{:S(2)}) collective-permute-start(bf16[640,512]{1,0:T(8,128)(2,1)S(1)} %copy-done.29), channel_id=1, source_target_pairs={{0,4},{4,0},{8,12},{12,8},{16,20},{20,16},{24,28},{28,24},{1,5},{5... | collective-permute-start | bytes 1966088 | tf_op jit(solution)/shard_map/ppermute | solution.py:530
  55.5 52.2 %collective-permute-start.39 = (bf16[128,2048]{1,0:T(8,128)(2,1)S(1)}, bf16[128,2048]{1,0:T(8,128)(2,1)S(1)}, u32[]{:S(2)}, u32[]{:S(2)}) collective-permute-start(bf16[128,2048]{1,0:T(8,128)(2,1)S(1)} %copy-done.4), channel_id=1, source_target_pairs={{0,2},{1,3},{2,0},{3,1},{4,6},{5,7},{6,4},{7,5},{8,10},{9,11},{10,... | collective-permute-start | bytes 1572872 | tf_op jit(solution)/shard_map/ppermute | solution.py:536
  57.3 32.7 %collective-permute-start.55 = (bf16[256,704]{1,0:T(8,128)(2,1)S(1)}, bf16[256,704]{1,0:T(8,128)(2,1)S(1)}, u32[]{:S(2)}, u32[]{:S(2)}) collective-permute-start(bf16[256,704]{1,0:T(8,128)(2,1)S(1)} %get-tuple-element.23), channel_id=1, source_target_pairs={{0,4},{4,0},{8,12},{12,8},{16,20},{20,16},{24,28},{28,24},{1,5},{5... | collective-permute-start | bytes 1081352 | tf_op jit(solution)/shard_map/ppermute | solution.py:530
  58.8 31.4 %collective-permute-start.56 = (bf16[256,704]{1,0:T(8,128)(2,1)S(1)}, bf16[256,704]{1,0:T(8,128)(2,1)S(1)}, u32[]{:S(2)}, u32[]{:S(2)}) collective-permute-start(bf16[256,704]{1,0:T(8,128)(2,1)S(1)} %get-tuple-element.24.refs_0_), channel_id=1, source_target_pairs={{0,8},{4,12},{8,16},{12,20},{16,24},{20,28},{24,0},{28,4},{1,9},{5... | collective-permute-start | bytes 1081352 | tf_op jit(solution)/shard_map/ppermute | solution.py:533
  58.8 30.5 %collective-permute-start.38 = (f32[1,1024]{1,0:T(1,128)S(1)}, f32[1,1024]{1,0:T(1,128)S(1)}, u32[]{:S(2)}, u32[]{:S(2)}) collective-permute-start(f32[1,1024]{1,0:T(1,128)S(1)} %pad_maximum_fusion.12), channel_id=1, source_target_pairs={{0,1},{1,0},{2,3},{3,2},{4,5},{5,4},{6,7},{7,6},{8,9},{9,8},{10,11... | collective-permute-start | bytes 12296 | tf_op jit(solution)/shard_map/ppermute | solution.py:536
  89.4 17.4 %collective-permute-start.28 = (bf16[640,256]{1,0:T(8,128)(2,1)S(1)}, bf16[640,256]{1,0:T(8,128)(2,1)S(1)}, u32[]{:S(2)}, u32[]{:S(2)}) collective-permute-start(bf16[640,256]{1,0:T(8,128)(2,1)S(1)} %get-tuple-element.10), channel_id=1, source_target_pairs={{0,4},{4,0},{8,12},{12,8},{16,20},{20,16},{24,28},{28,24},{1,5},{5... | collective-permute-start | bytes 983048 | tf_op jit(solution)/shard_map/ppermute | solution.py:530
  90.0 31.4 %collective-permute-start.40 = (bf16[128,2048]{1,0:T(8,128)(2,1)S(1)}, bf16[128,2048]{1,0:T(8,128)(2,1)S(1)}, u32[]{:S(2)}, u32[]{:S(2)}) collective-permute-start(bf16[128,2048]{1,0:T(8,128)(2,1)S(1)} %copy-done.4), channel_id=1, source_target_pairs={{0,1},{1,0},{2,3},{3,2},{4,5},{5,4},{6,7},{7,6},{8,9},{9,8},{10,11... | collective-permute-start | bytes 1572872 | tf_op jit(solution)/shard_map/ppermute | solution.py:536
  90.2 33.4 %collective-permute-start.48 = (bf16[256,1408]{1,0:T(8,128)(2,1)S(1)}, bf16[256,1408]{1,0:T(8,128)(2,1)S(1)}, u32[]{:S(2)}, u32[]{:S(2)}) collective-permute-start(bf16[256,1408]{1,0:T(8,128)(2,1)S(1)} %get-tuple-element.19), channel_id=1, source_target_pairs={{0,4},{4,0},{8,12},{12,8},{16,20},{20,16},{24,28},{28,24},{1,5},{5... | collective-permute-start | bytes 2162696 | tf_op jit(solution)/shard_map/ppermute | solution.py:530
  106.8 22.2 %collective-permute-start.49 = (bf16[256,1408]{1,0:T(8,128)(2,1)S(1)}, bf16[256,1408]{1,0:T(8,128)(2,1)S(1)}, u32[]{:S(2)}, u32[]{:S(2)}) collective-permute-start(bf16[256,1408]{1,0:T(8,128)(2,1)S(1)} %get-tuple-element.20.refs_0_), channel_id=1, source_target_pairs={{0,8},{4,12},{8,16},{12,20},{16,24},{20,28},{24,0},{28,4},{1,9},{5... | collective-permute-start | bytes 2162696 | tf_op jit(solution)/shard_map/ppermute | solution.py:533
  107.8 21.8 %collective-permute-start.29 = (bf16[1280,256]{1,0:T(8,128)(2,1)S(1)}, bf16[1280,256]{1,0:T(8,128)(2,1)S(1)}, u32[]{:S(2)}, u32[]{:S(2)}) collective-permute-start(bf16[1280,256]{1,0:T(8,128)(2,1)S(1)} %maximum_select_fusion.1), channel_id=1, source_target_pairs={{0,2},{1,3},{2,0},{3,1},{4,6},{5,7},{6,4},{7,5},{8,10},{9,11},{10,... | collective-permute-start | bytes 1966088 | tf_op jit(solution)/shard_map/ppermute | solution.py:536
  121.4 61.4 %collective-permute-start.31 = (bf16[256,2048]{1,0:T(8,128)(2,1)}, bf16[256,2048]{1,0:T(8,128)(2,1)}, u32[]{:S(2)}, u32[]{:S(2)}) collective-permute-start(bf16[256,2048]{1,0:T(8,128)(2,1)} %refs_1_.1), channel_id=1, source_target_pairs={{0,2},{1,3},{2,0},{3,1},{4,6},{5,7},{6,4},{7,5},{8,10},{9,11},{10,... | collective-permute-start | bytes 3145736 | tf_op jit(solution)/shard_map/ppermute | solution.py:536
  123.7 61.1 %collective-permute-start.32 = (bf16[256,2048]{1,0:T(8,128)(2,1)}, bf16[256,2048]{1,0:T(8,128)(2,1)}, u32[]{:S(2)}, u32[]{:S(2)}) collective-permute-start(bf16[256,2048]{1,0:T(8,128)(2,1)} %refs_1_.1), channel_id=1, source_target_pairs={{0,1},{1,0},{2,3},{3,2},{4,5},{5,4},{6,7},{7,6},{8,9},{9,8},{10,11... | collective-permute-start | bytes 3145736 | tf_op jit(solution)/shard_map/ppermute | solution.py:536
  127.3 61.3 %collective-permute-start.43 = (bf16[1280,512]{1,0:T(8,128)(2,1)S(1)}, bf16[1280,512]{1,0:T(8,128)(2,1)}, u32[]{:S(2)}, u32[]{:S(2)}) collective-permute-start(bf16[1280,512]{1,0:T(8,128)(2,1)S(1)} %maximum_select_fusion.refs_7_), channel_id=1, source_target_pairs={{0,2},{1,3},{2,0},{3,1},{4,6},{5,7},{6,4},{7,5},{8,10},{9,11},{10,... | collective-permute-start | bytes 3932168 | tf_op jit(solution)/shard_map/ppermute | solution.py:536
  129.0 52.9 %collective-permute-start.35 = (bf16[1280,128]{1,0:T(8,128)(2,1)S(1)}, bf16[1280,128]{1,0:T(8,128)(2,1)S(1)}, u32[]{:S(2)}, u32[]{:S(2)}) collective-permute-start(bf16[1280,128]{1,0:T(8,128)(2,1)S(1)} %maximum_select_fusion.2), channel_id=1, source_target_pairs={{0,2},{1,3},{2,0},{3,1},{4,6},{5,7},{6,4},{7,5},{8,10},{9,11},{10,... | collective-permute-start | bytes 983048 | tf_op jit(solution)/shard_map/ppermute | solution.py:536
  129.6 53.8 %collective-permute-start.57 = (bf16[256,704]{1,0:T(8,128)(2,1)S(1)}, bf16[256,704]{1,0:T(8,128)(2,1)S(1)}, u32[]{:S(2)}, u32[]{:S(2)}) collective-permute-start(bf16[256,704]{1,0:T(8,128)(2,1)S(1)} %collective-permute-done.55.refs_1_), channel_id=1, source_target_pairs={{0,8},{4,12},{8,16},{12,20},{16,24},{20,28},{24,0},{28,4},{1,9},{5... | collective-permute-start | bytes 1081352 | tf_op jit(solution)/shard_map/ppermute | solution.py:533
  181.8 25.5 %collective-permute-start.30 = (bf16[1280,512]{1,0:T(8,128)(2,1)}, bf16[1280,512]{1,0:T(8,128)(2,1)}, u32[]{:S(2)}, u32[]{:S(2)}) collective-permute-start(bf16[1280,512]{1,0:T(8,128)(2,1)} %pad_maximum_fusion.1), channel_id=1, source_target_pairs={{0,1},{1,0},{2,3},{3,2},{4,5},{5,4},{6,7},{7,6},{8,9},{9,8},{10,11... | collective-permute-start | bytes 3932168 | tf_op jit(solution)/shard_map/ppermute | solution.py:536
  182.8 22.5 %collective-permute-start.33 = (bf16[256,2048]{1,0:T(8,128)(2,1)}, bf16[256,2048]{1,0:T(8,128)(2,1)}, u32[]{:S(2)}, u32[]{:S(2)}) collective-permute-start(bf16[256,2048]{1,0:T(8,128)(2,1)} %collective-permute-done.31.refs_2_), channel_id=1, source_target_pairs={{0,1},{1,0},{2,3},{3,2},{4,5},{5,4},{6,7},{7,6},{8,9},{9,8},{10,11... | collective-permute-start | bytes 3145736 | tf_op jit(solution)/shard_map/ppermute | solution.py:536
  184.8 20.5 %collective-permute-start.50 = (bf16[256,1408]{1,0:T(8,128)(2,1)}, bf16[256,1408]{1,0:T(8,128)(2,1)S(1)}, u32[]{:S(2)}, u32[]{:S(2)}) collective-permute-start(bf16[256,1408]{1,0:T(8,128)(2,1)} %copy-done.35), channel_id=1, source_target_pairs={{0,8},{4,12},{8,16},{12,20},{16,24},{20,28},{24,0},{28,4},{1,9},{5... | collective-permute-start | bytes 2162696 | tf_op jit(solution)/shard_map/ppermute | solution.py:533
  188.6 37.9 %collective-permute-start.44 = (bf16[1280,512]{1,0:T(8,128)(2,1)S(1)}, bf16[1280,512]{1,0:T(8,128)(2,1)S(1)}, u32[]{:S(2)}, u32[]{:S(2)}) collective-permute-start(bf16[1280,512]{1,0:T(8,128)(2,1)S(1)} %maximum_select_fusion.refs_7_), channel_id=1, source_target_pairs={{0,1},{1,0},{2,3},{3,2},{4,5},{5,4},{6,7},{7,6},{8,9},{9,8},{10,11... | collective-permute-start | bytes 3932168 | tf_op jit(solution)/shard_map/ppermute | solution.py:536
  188.7 53.2 %collective-permute-start.45 = (bf16[1280,512]{1,0:T(8,128)(2,1)}, bf16[1280,512]{1,0:T(8,128)(2,1)S(1)}, u32[]{:S(2)}, u32[]{:S(2)}) collective-permute-start(bf16[1280,512]{1,0:T(8,128)(2,1)} %collective-permute-done.43.refs_8_), channel_id=1, source_target_pairs={{0,1},{1,0},{2,3},{3,2},{4,5},{5,4},{6,7},{7,6},{8,9},{9,8},{10,11... | collective-permute-start | bytes 3932168 | tf_op jit(solution)/shard_map/ppermute | solution.py:536
  205.3 12.8 %collective-permute-start.41 = (bf16[128,2048]{1,0:T(8,128)(2,1)S(1)}, bf16[128,2048]{1,0:T(8,128)(2,1)S(1)}, u32[]{:S(2)}, u32[]{:S(2)}) collective-permute-start(bf16[128,2048]{1,0:T(8,128)(2,1)S(1)} %collective-permute-done.39.refs_4_), channel_id=1, source_target_pairs={{0,1},{1,0},{2,3},{3,2},{4,5},{5,4},{6,7},{7,6},{8,9},{9,8},{10,11... | collective-permute-start | bytes 1572872 | tf_op jit(solution)/shard_map/ppermute | solution.py:536
  205.4 21.0 %collective-permute-start.51 = (bf16[256,1408]{1,0:T(8,128)(2,1)S(1)}, bf16[256,1408]{1,0:T(8,128)(2,1)}, u32[]{:S(2)}, u32[]{:S(2)}) collective-permute-start(bf16[256,1408]{1,0:T(8,128)(2,1)S(1)} %copy-done.37), channel_id=1, source_target_pairs={{0,8},{4,12},{8,16},{12,20},{16,24},{20,28},{24,0},{28,4},{1,9},{5... | collective-permute-start | bytes 2162696 | tf_op jit(solution)/shard_map/ppermute | solution.py:533
  207.3 34.4 %collective-permute-start.52 = (bf16[256,1408]{1,0:T(8,128)(2,1)S(1)}, bf16[256,1408]{1,0:T(8,128)(2,1)}, u32[]{:S(2)}, u32[]{:S(2)}) collective-permute-start(bf16[256,1408]{1,0:T(8,128)(2,1)S(1)} %collective-permute-done.50.refs_3_), channel_id=1, source_target_pairs={{0,8},{4,12},{8,16},{12,20},{16,24},{20,28},{24,0},{28,4},{1,9},{5... | collective-permute-start | bytes 2162696 | tf_op jit(solution)/shard_map/ppermute | solution.py:533
  218.1 38.9 %collective-permute-start.58 = (bf16[256,704]{1,0:T(8,128)(2,1)S(1)}, bf16[256,704]{1,0:T(8,128)(2,1)S(1)}, u32[]{:S(2)}, u32[]{:S(2)}) collective-permute-start(bf16[256,704]{1,0:T(8,128)(2,1)S(1)} %collective-permute-done.56.refs_2_), channel_id=1, source_target_pairs={{0,8},{4,12},{8,16},{12,20},{16,24},{20,28},{24,0},{28,4},{1,9},{5... | collective-permute-start | bytes 1081352 | tf_op jit(solution)/shard_map/ppermute | solution.py:533
  226.3 36.3 %collective-permute-start.59 = (bf16[256,704]{1,0:T(8,128)(2,1)S(1)}, bf16[256,704]{1,0:T(8,128)(2,1)}, u32[]{:S(2)}, u32[]{:S(2)}) collective-permute-start(bf16[256,704]{1,0:T(8,128)(2,1)S(1)} %collective-permute-done.57.refs_3_), channel_id=1, source_target_pairs={{0,8},{4,12},{8,16},{12,20},{16,24},{20,28},{24,0},{28,4},{1,9},{5... | collective-permute-start | bytes 1081352 | tf_op jit(solution)/shard_map/ppermute | solution.py:533
  226.5 64.4 %collective-permute-start.53 = (bf16[256,1408]{1,0:T(8,128)(2,1)}, bf16[256,1408]{1,0:T(8,128)(2,1)}, u32[]{:S(2)}, u32[]{:S(2)}) collective-permute-start(bf16[256,1408]{1,0:T(8,128)(2,1)} %collective-permute-done.51.refs_4_), channel_id=1, source_target_pairs={{0,8},{4,12},{8,16},{12,20},{16,24},{20,28},{24,0},{28,4},{1,9},{5... | collective-permute-start | bytes 2162696 | tf_op jit(solution)/shard_map/ppermute | solution.py:533
  241.8 49.0 %collective-permute-start.54 = (bf16[256,1408]{1,0:T(8,128)(2,1)}, bf16[256,1408]{1,0:T(8,128)(2,1)}, u32[]{:S(2)}, u32[]{:S(2)}) collective-permute-start(bf16[256,1408]{1,0:T(8,128)(2,1)} %collective-permute-done.52.refs_5_), channel_id=1, source_target_pairs={{0,8},{4,12},{8,16},{12,20},{16,24},{20,28},{24,0},{28,4},{1,9},{5... | collective-permute-start | bytes 2162696 | tf_op jit(solution)/shard_map/ppermute | solution.py:533
  255.7 33.9 %collective-permute-start.46 = (bf16[1,2048]{1,0:T(2,128)(2,1)S(1)}, bf16[1,2048]{1,0:T(2,128)(2,1)S(1)}, u32[]{:S(2)}, u32[]{:S(2)}) collective-permute-start(bf16[1,2048]{1,0:T(2,128)(2,1)S(1)} %get-tuple-element.37), channel_id=1, source_target_pairs={{8,0},{12,4},{16,8},{20,12},{24,16},{28,20},{9,1},{13,5},{17,9},{2... | collective-permute-start | bytes 12296 | tf_op jit(solution)/shard_map/ppermute | solution.py:656
  257.0 33.1 %collective-permute-start.47 = (bf16[1,2048]{1,0:T(2,128)(2,1)S(1)}, bf16[1,2048]{1,0:T(2,128)(2,1)S(1)}, u32[]{:S(2)}, u32[]{:S(2)}) collective-permute-start(bf16[1,2048]{1,0:T(2,128)(2,1)S(1)} %get-tuple-element.38), channel_id=1, source_target_pairs={{0,8},{4,12},{8,16},{12,20},{16,24},{20,28},{1,9},{5,13},{9,17},{1... | collective-permute-start | bytes 12296 | tf_op jit(solution)/shard_map/ppermute | solution.py:655
  262.6 47.8 %collective-permute-start.60 = (bf16[256,704]{1,0:T(8,128)(2,1)S(1)}, bf16[256,704]{1,0:T(8,128)(2,1)S(1)}, u32[]{:S(2)}, u32[]{:S(2)}) collective-permute-start(bf16[256,704]{1,0:T(8,128)(2,1)S(1)} %collective-permute-done.58.refs_4_), channel_id=1, source_target_pairs={{0,8},{4,12},{8,16},{12,20},{16,24},{20,28},{24,0},{28,4},{1,9},{5... | collective-permute-start | bytes 1081352 | tf_op jit(solution)/shard_map/ppermute | solution.py:533
  289.6 20.9 %collective-permute-start.61 = (bf16[256,704]{1,0:T(8,128)(2,1)}, bf16[256,704]{1,0:T(8,128)(2,1)S(1)}, u32[]{:S(2)}, u32[]{:S(2)}) collective-permute-start(bf16[256,704]{1,0:T(8,128)(2,1)} %collective-permute-done.59.refs_5_), channel_id=1, source_target_pairs={{0,8},{4,12},{8,16},{12,20},{16,24},{20,28},{24,0},{28,4},{1,9},{5... | collective-permute-start | bytes 1081352 | tf_op jit(solution)/shard_map/ppermute | solution.py:533
  323.8 28.3 %collective-permute-start.63 = (bf16[2,320,512]{2,1,0:T(8,128)(2,1)S(1)}, bf16[2,320,512]{2,1,0:T(8,128)(2,1)S(1)}, u32[]{:S(2)}, u32[]{:S(2)}) collective-permute-start(bf16[2,320,512]{2,1,0:T(8,128)(2,1)S(1)} %slice_bitcast_fusion.1), channel_id=1, source_target_pairs={{0,4},{4,0},{8,12},{12,8},{16,20},{20,16},{24,28},{28,24},{1,5},{5... | collective-permute-start | bytes 1966088 | tf_op jit(solution)/shard_map/ppermute | solution.py:530
  336.7 16.9 %collective-permute-start.65 = (bf16[2,320,512]{2,1,0:T(8,128)(2,1)S(1)}, bf16[2,320,512]{2,1,0:T(8,128)(2,1)S(1)}, u32[]{:S(2)}, u32[]{:S(2)}) collective-permute-start(bf16[2,320,512]{2,1,0:T(8,128)(2,1)S(1)} %slice_bitcast_fusion), channel_id=1, source_target_pairs={{0,2},{1,3},{2,0},{3,1},{4,6},{5,7},{6,4},{7,5},{8,10},{9,11},{10,... | collective-permute-start | bytes 1966088 | tf_op jit(solution)/shard_map/ppermute | solution.py:536
  353.7 9.0 %collective-permute-start.64 = (bf16[320,512]{1,0:T(8,128)(2,1)S(1)}, bf16[320,512]{1,0:T(8,128)(2,1)S(1)}, u32[]{:S(2)}, u32[]{:S(2)}) collective-permute-start(bf16[320,512]{1,0:T(8,128)(2,1)S(1)} %get-tuple-element.17), channel_id=1, source_target_pairs={{0,2},{1,3},{2,0},{3,1},{4,6},{5,7},{6,4},{7,5},{8,10},{9,11},{10,... | collective-permute-start | bytes 983048 | tf_op jit(solution)/shard_map/ppermute | solution.py:536
  355.1 8.7 %collective-permute-start.66 = (bf16[320,512]{1,0:T(8,128)(2,1)S(1)}, bf16[320,512]{1,0:T(8,128)(2,1)S(1)}, u32[]{:S(2)}, u32[]{:S(2)}) collective-permute-start(bf16[320,512]{1,0:T(8,128)(2,1)S(1)} %get-tuple-element.18), channel_id=1, source_target_pairs={{0,4},{4,0},{8,12},{12,8},{16,20},{20,16},{24,28},{28,24},{1,5},{5... | collective-permute-start | bytes 983048 | tf_op jit(solution)/shard_map/ppermute | solution.py:530
  (58 other events, 958.7 us)
